TPU v7x, 32 devices: a whole 2x2x4 slice. The times are simulated.
32 devices in a mesh: sp: 8 (over z, x), tp: 4 (over y, core).
Axes of the slice: x: 2, y: 2, z: 4, core: 2. Of those that a mesh axis runs over, the one named last changes fastest.
Arguments:
- queries: bfloat16 [2560, 1024], P('sp', 'tp'), may hold values from -6.6 to 6.6
- key_matrix: bfloat16 [2560, 256], P('sp', 'tp'), may hold values from -6.6 to 6.6
- values: bfloat16 [2560, 256], P('sp', 'tp'), may hold values from -6 to 6
- query_gain: float32 [64], replicated, may hold values from 0.19 to 8
- key_norm_gain: float32 [64], replicated, may hold values from 0.19 to 8
- head_gain: float32 [1024], P('tp'), may hold values from 0.1 to 1.9
- out_proj: bfloat16 [1024, 2048], replicated, may hold values from -0.1875 to 0.1875
- residual: bfloat16 [2560, 2048], P('sp'), may hold values from -6 to 6
- ffn_gain: float32 [2048], replicated, may hold values from 0.1 to 1.9
- routes: int32 [2560, 4], P('sp'), may hold values from 0 to 31, all different within a row; in each aligned block of 320 rows (0 to 319, 320 to 639, ...) at most 80 rows name the same one
- route_weights: float32 [2560, 4], P('sp'), may hold values from 0.2 to 1
- expert_gate: bfloat16 [32, 2048, 512], P(('sp', 'tp')), may hold values from -0.125 to 0.125
- expert_up: bfloat16 [32, 2048, 512], P(('sp', 'tp')), may hold values from -0.125 to 0.125
- expert_down: bfloat16 [32, 512, 2048], P(('sp', 'tp')), may hold values from -0.25 to 0.25
- shared_gate: bfloat16 [2048, 512], P(None, 'tp'), may hold values from -0.125 to 0.125
- shared_up: bfloat16 [2048, 512], P(None, 'tp'), may hold values from -0.125 to 0.125
- shared_down: bfloat16 [512, 2048], P('tp'), may hold values from -0.25 to 0.25
Outputs:
- layer_out: bfloat16 [2560, 2048], P(('sp', 'tp'))
Inputs may be any that keep to these rules, and one draw needn't show every extreme that they name: `routes`: each row names 4 different experts; in each aligned block of 320 rows (the tokens of one index of sp) no expert is named more than 80 times, a bound that some block reaches.
All inputs are finite; a program needn't handle non-finite values.
Results may differ from a plain program's by a relative error of at most 0.019.
The roundings to bfloat16 on the way count: a program that leaves them out, or rounds other values in their place, can miss the bound.
Values may be sent and summed in bfloat16 or wider, within the bound.
A program may use at most 128 MiB of HBM per device.

v0:
```python
import jax
import jax.numpy as jnp
from jax import lax
from jax.experimental import pallas as pl
from jax.experimental.pallas import tpu as pltpu
from jax.sharding import PartitionSpec as P

HEAD_SIZE = 64
GRID_W = 64


EPS = 1e-06
THETA = 10000.0


def final_norm(field, gain):
    mean_sq = jnp.mean(field * field, axis=-1, keepdims=True)
    return field * lax.rsqrt(mean_sq + EPS) * gain


def grid_tables(positions, sequence_total):
    grid_rows = sequence_total // GRID_W
    row_pos = (positions // GRID_W - grid_rows // 2).astype(jnp.float32)
    col_pos = (positions % GRID_W - GRID_W // 2).astype(jnp.float32)
    quarter = HEAD_SIZE // 4
    inverse = THETA ** (-jnp.arange(quarter, dtype=jnp.float32) / quarter)
    angles = jnp.concatenate([row_pos[:, None] * inverse, col_pos[:, None] * inverse], axis=1)
    return (jnp.cos(angles), jnp.sin(angles))


def apply_rotary(field, cosine_table, sine_table):
    row_count, head_count = (field.shape[0], field.shape[1])
    quarter = HEAD_SIZE // 4
    pieces = field.reshape(row_count, head_count, 2, 2, quarter)
    front_half = pieces[:, :, :, 0, :].reshape(row_count, head_count, 2 * quarter)
    back_half = pieces[:, :, :, 1, :].reshape(row_count, head_count, 2 * quarter)
    cos_wide = cosine_table[:, None, :]
    sin_wide = sine_table[:, None, :]
    new_front = (front_half * cos_wide - back_half * sin_wide).reshape(
        row_count, head_count, 2, 1, quarter
    )
    new_back = (front_half * sin_wide + back_half * cos_wide).reshape(
        row_count, head_count, 2, 1, quarter
    )
    return jnp.concatenate([new_front, new_back], axis=3).reshape(row_count, head_count, HEAD_SIZE)


def exchange(block, axis, call_id, gather):
    count = lax.axis_size(axis)
    if count == 1:
        return block[None] if gather else block
    shape = (count,) + block.shape if gather else block.shape

    def kernel(in_ref, out_ref, send_sems, recv_sems, own_sem):
        me = lax.axis_index(axis)
        barrier = pltpu.get_barrier_semaphore()
        for step in range(1, count):
            pl.semaphore_signal(
                barrier,
                inc=1,
                device_id={axis: lax.rem(me + step, count)},
                device_id_type=pl.DeviceIdType.MESH,
            )
        own = pltpu.make_async_copy(in_ref if gather else in_ref.at[me], out_ref.at[me], own_sem)
        own.start()
        pl.semaphore_wait(barrier, count - 1)
        copies = []
        for step in range(1, count):
            peer = lax.rem(me + step, count)
            copy = pltpu.make_async_remote_copy(
                src_ref=in_ref if gather else in_ref.at[peer],
                dst_ref=out_ref.at[me],
                send_sem=send_sems.at[step],
                recv_sem=recv_sems.at[step],
                device_id={axis: peer},
                device_id_type=pl.DeviceIdType.MESH,
            )
            copy.start()
            copies.append(copy)
        own.wait()
        for copy in copies:
            copy.wait()

    return pl.pallas_call(
        kernel,
        out_shape=jax.ShapeDtypeStruct(shape, block.dtype),
        in_specs=[pl.BlockSpec(memory_space=pltpu.VMEM)],
        out_specs=pl.BlockSpec(memory_space=pltpu.VMEM),
        scratch_shapes=[
            pltpu.SemaphoreType.DMA((count,)),
            pltpu.SemaphoreType.DMA((count,)),
            pltpu.SemaphoreType.DMA,
        ],
        compiler_params=pltpu.CompilerParams(collective_id=call_id, has_side_effects=True),
        name="exchange_%d" % call_id,
    )(block)


def key_block_rows(piece_rows):
    return max((width for width in range(1, 2049) if piece_rows % width == 0))


MESH = pl.DeviceIdType.MESH
COLUMNS = 512


def proxy_plane(t):
    pair, side = t // 2, t % 2
    return pair + side * (3 - 2 * pair)


def proxy_of(plane):
    return jnp.where(plane == 0, 0, jnp.where(plane == 3, 1, plane + 1))


def place(planes, width, tp_count):
    sp, t = lax.axis_index("sp"), lax.axis_index("tp")
    z, x = sp // width, sp % width
    return z, x, t, x * tp_count + t


def greet(z, x, p, planes, width, tp_count):
    barrier = pltpu.get_barrier_semaphore()
    group = width * tp_count
    for step in range(1, group):
        peer = lax.rem(p + step, group)
        pl.semaphore_signal(
            barrier,
            inc=1,
            device_id={"sp": z * width + peer // tp_count, "tp": peer % tp_count},
            device_id_type=MESH,
        )
    for step in (1, planes - 1):
        pl.semaphore_signal(
            barrier,
            inc=1,
            device_id={"sp": lax.rem(z + step, planes) * width + x},
            device_id_type=MESH,
        )
    pl.semaphore_wait(barrier, group - 1 + 2)


def dispatch(normed_own, select, shards, planes, width, tp_count, call_id):
    rows, model = normed_own.shape
    group, capacity, tokens = select.shape
    quarters = tokens // rows

    given = len(shards)

    def kernel(own_ref, sel_ref, *refs):
        shard_refs, out_ref, pair_refs = refs[:given], refs[given], refs[given + 1 : 2 * given + 1]
        blk, packed, a_send, z_send, b_recv, c_send, c_recv, w_send, w_recv, sem = refs[
            2 * given + 1 :
        ]
        z, x, t, p = place(planes, width, tp_count)
        zb = proxy_plane(t)
        home = z == zb
        greet(z, x, p, planes, width, tp_count)
        target = proxy_of(z)

        def to_home():
            return pltpu.make_async_remote_copy(
                src_ref=own_ref,
                dst_ref=blk.at[t],
                send_sem=a_send,
                recv_sem=b_recv.at[t],
                device_id={"tp": target},
                device_id_type=MESH,
            )

        @pl.when(t != target)
        def _():
            to_home().start()

        pairs = [
            pltpu.make_async_remote_copy(
                src_ref=shard_refs[i],
                dst_ref=pair_refs[i],
                send_sem=w_send.at[i],
                recv_sem=w_recv.at[i],
                device_id={"tp": t + 1 - 2 * lax.rem(t, 2)},
                device_id_type=MESH,
            )
            for i in range(given)
        ]
        for copy in pairs:
            copy.start()
        own_copy = pltpu.make_async_copy(own_ref, blk.at[t], sem)

        @pl.when(home)
        def _():
            own_copy.start()
            own_copy.wait()

        def relay(q, up):
            return pltpu.make_async_remote_copy(
                src_ref=blk.at[q],
                dst_ref=blk.at[q],
                send_sem=z_send.at[up, q],
                recv_sem=b_recv.at[q],
                device_id={"sp": (z + (1 if up else -1)) * width + x},
                device_id_type=MESH,
            )

        go_up = (z >= zb) & (z < planes - 1)
        go_down = (z <= zb) & (z > 0)

        for k in range(quarters):
            q = lax.rem(t + k, quarters)

            @pl.when(jnp.logical_not(home & (q == t)))
            def _():
                relay(q, 1).wait_recv()

            @pl.when(go_up)
            def _():
                relay(q, 1).start()

            @pl.when(go_down)
            def _():
                relay(q, 0).start()

        def send(pp):
            return pltpu.make_async_remote_copy(
                src_ref=packed.at[pp],
                dst_ref=out_ref.at[zb * width + x],
                send_sem=c_send.at[pp],
                recv_sem=c_recv.at[zb * width + x],
                device_id={"sp": z * width + pp // tp_count, "tp": pp % tp_count},
                device_id_type=MESH,
            )

        def serve(k, carry):
            pp = lax.rem(p + 1 + k, group)
            chosen = sel_ref[pp]
            for column in range(0, model, COLUMNS):
                part = pl.ds(column, COLUMNS)
                packed[pp, :, part] = jnp.dot(
                    chosen,
                    blk[:, :, part].reshape(tokens, COLUMNS),
                    preferred_element_type=jnp.float32,
                ).astype(jnp.bfloat16)

            @pl.when(pp != p)
            def _():
                send(pp).start()

            return carry

        lax.fori_loop(0, group, serve, 0)
        kept = pltpu.make_async_copy(packed.at[p], out_ref.at[zb * width + x], sem)
        kept.start()
        kept.wait()

        def finish(k, carry):
            pp = lax.rem(p + 1 + k, group)
            send(pp).wait_send()
            source = proxy_plane(pp % tp_count) * width + pp // tp_count
            pltpu.make_async_remote_copy(
                src_ref=packed.at[pp],
                dst_ref=out_ref.at[source],
                send_sem=c_send.at[pp],
                recv_sem=c_recv.at[source],
                device_id={"sp": z * width + pp // tp_count, "tp": pp % tp_count},
                device_id_type=MESH,
            ).wait_recv()
            return carry

        lax.fori_loop(0, group - 1, finish, 0)

        @pl.when(t != target)
        def _():
            to_home().wait_send()

        for q in range(quarters):

            @pl.when(go_up)
            def _():
                relay(q, 1).wait_send()

            @pl.when(go_down)
            def _():
                relay(q, 0).wait_send()

        for copy in pairs:
            copy.wait()

    vmem = pl.BlockSpec(memory_space=pltpu.VMEM)
    dma = pltpu.SemaphoreType.DMA
    return pl.pallas_call(
        kernel,
        out_shape=[jax.ShapeDtypeStruct((planes * width, capacity, model), jnp.bfloat16)]
        + [jax.ShapeDtypeStruct(w.shape, w.dtype) for w in shards],
        in_specs=[vmem] * 2 + [pl.BlockSpec(memory_space=pl.ANY)] * given,
        out_specs=[vmem] + [pl.BlockSpec(memory_space=pl.ANY)] * given,
        scratch_shapes=[
            pltpu.VMEM((quarters, rows, model), jnp.bfloat16),
            pltpu.VMEM((group, capacity, model), jnp.bfloat16),
            dma,
            dma((2, quarters)),
            dma((quarters,)),
            dma((group,)),
            dma((planes * width,)),
            dma((given,)),
            dma((given,)),
            dma,
        ],
        compiler_params=pltpu.CompilerParams(collective_id=call_id, has_side_effects=True),
        name="dispatch",
    )(normed_own, select, *shards)


def give_back(produced, weights_hi, weights_lo, own, shards, planes, width, tp_count, call_id):
    blocks, capacity, model = produced.shape
    group, quarters = width * tp_count, tp_count
    slots, tokens = weights_hi.shape
    rows = tokens // quarters

    pieces = len(shards) // 3

    def kernel(in_ref, hi_ref, lo_ref, own_ref, *refs):
        gates, ups = refs[:pieces], refs[pieces : 2 * pieces]
        downs, refs = refs[2 * pieces : 3 * pieces], refs[3 * pieces :]
        out_ref, shared_ref, back, high, low, total, passed, arrived = refs[:8]
        c_send, c_recv, z_send, z_recv, a_recv, sem = refs[8:]
        z, x, t, p = place(planes, width, tp_count)
        zb = proxy_plane(t)
        home = z == zb
        greet(z, x, p, planes, width, tp_count)
        keep = pltpu.make_async_copy(in_ref.at[zb * width + x], back.at[p], sem)
        keep.start()

        def send(pp):
            return pltpu.make_async_remote_copy(
                src_ref=in_ref.at[proxy_plane(pp % tp_count) * width + pp // tp_count],
                dst_ref=back.at[p],
                send_sem=c_send.at[pp],
                recv_sem=c_recv.at[p],
                device_id={"sp": z * width + pp // tp_count, "tp": pp % tp_count},
                device_id_type=MESH,
            )

        def came(pp):
            return pltpu.make_async_remote_copy(
                src_ref=in_ref.at[0],
                dst_ref=back.at[pp],
                send_sem=c_send.at[pp],
                recv_sem=c_recv.at[pp],
                device_id={"sp": z * width + pp // tp_count, "tp": pp % tp_count},
                device_id_type=MESH,
            )

        def issue(k, carry):
            rank = k // width
            plane = jnp.where(2 * z < planes, planes - 1 - rank, rank)
            pp = lax.rem(x + k + 1, width) * tp_count + proxy_of(plane)

            @pl.when(pp != p)
            def _():
                send(pp).start()

            return carry

        lax.fori_loop(0, group, issue, 0)
        high[...] = hi_ref[...].T.reshape(quarters, rows, slots)
        low[...] = lo_ref[...].T.reshape(quarters, rows, slots)
        for i in range(pieces):
            gate = jnp.dot(own_ref[...], gates[i][...], preferred_element_type=jnp.float32)
            up = jnp.dot(own_ref[...], ups[i][...], preferred_element_type=jnp.float32)
            inner = (gate / (1.0 + jnp.exp(-gate)) * up).astype(jnp.bfloat16)
            for column in range(0, model, COLUMNS):
                part = pl.ds(column, COLUMNS)
                share = jnp.dot(inner, downs[i][:, part], preferred_element_type=jnp.float32)
                if i == 0:
                    shared_ref[:, part] = share
                else:
                    shared_ref[:, part] += share
        keep.wait()

        def collect(k, carry):
            came(lax.rem(p + 1 + k, group)).wait_recv()
            return carry

        lax.fori_loop(0, group - 1, collect, 0)

        from_above = (z >= zb) & (z < planes - 1)
        from_below = (z <= zb) & (z > 0)

        def hop(q, down):
            return pltpu.make_async_remote_copy(
                src_ref=passed.at[q],
                dst_ref=arrived.at[down, q],
                send_sem=z_send.at[q],
                recv_sem=z_recv.at[down, q],
                device_id={"sp": (z + (-1 if down else 1)) * width + x},
                device_id_type=MESH,
            )

        def to_owner(q):
            return pltpu.make_async_remote_copy(
                src_ref=passed.at[q],
                dst_ref=out_ref,
                send_sem=z_send.at[q],
                recv_sem=a_recv,
                device_id={"tp": q},
                device_id_type=MESH,
            )

        def quarter(q, carry):
            for column in range(0, model, COLUMNS):
                part = pl.ds(column, COLUMNS)
                piece = back[:, :, part].reshape(slots, COLUMNS)
                total[:, part] = jnp.dot(
                    high[q], piece, preferred_element_type=jnp.float32
                ) + jnp.dot(low[q], piece, preferred_element_type=jnp.float32)

            @pl.when(from_above)
            def _():
                hop(q, 1).wait_recv()
                total[...] += arrived[1, q].astype(jnp.float32)

            @pl.when(from_below)
            def _():
                hop(q, 0).wait_recv()
                total[...] += arrived[0, q].astype(jnp.float32)

            passed[q] = total[...].astype(jnp.bfloat16)

            @pl.when(z > zb)
            def _():
                hop(q, 1).start()

            @pl.when(z < zb)
            def _():
                hop(q, 0).start()

            @pl.when(home & (q != t))
            def _():
                to_owner(q).start()

            @pl.when(home & (q == t))
            def _():
                mine = pltpu.make_async_copy(passed.at[q], out_ref, sem)
                mine.start()
                mine.wait()

            return carry

        lax.fori_loop(0, quarters, quarter, 0)

        @pl.when(jnp.logical_not(home))
        def _():
            to_owner(t).wait_recv()

        def sent(k, carry):
            send(lax.rem(p + 1 + k, group)).wait_send()
            return carry

        lax.fori_loop(0, group - 1, sent, 0)

        def left(q, carry):
            @pl.when(jnp.logical_not(home & (q == t)))
            def _():
                to_owner(q).wait_send()

            return carry

        lax.fori_loop(0, quarters, left, 0)

    vmem = pl.BlockSpec(memory_space=pltpu.VMEM)
    dma = pltpu.SemaphoreType.DMA
    return pl.pallas_call(
        kernel,
        out_shape=(
            jax.ShapeDtypeStruct((rows, model), jnp.bfloat16),
            jax.ShapeDtypeStruct((rows, model), jnp.float32),
        ),
        in_specs=[vmem] * (4 + 3 * pieces),
        out_specs=(vmem, vmem),
        scratch_shapes=[
            pltpu.VMEM((group, capacity, model), jnp.bfloat16),
            pltpu.VMEM((quarters, rows, slots), jnp.bfloat16),
            pltpu.VMEM((quarters, rows, slots), jnp.bfloat16),
            pltpu.VMEM((rows, model), jnp.float32),
            pltpu.VMEM((quarters, rows, model), jnp.bfloat16),
            pltpu.VMEM((2, quarters, rows, model), jnp.bfloat16),
            dma((group,)),
            dma((group,)),
            dma((quarters,)),
            dma((2, quarters)),
            dma,
            dma,
        ],
        compiler_params=pltpu.CompilerParams(collective_id=call_id, has_side_effects=True),
        name="give_back",
    )(produced, weights_hi, weights_lo, own, *shards)


def attend(queries_t, own, gain, tokens, width, tp_count, call_id):
    count = lax.axis_size("sp")
    planes = count // width
    span = queries_t.shape[1]
    heads = gain.shape[0]
    chunk = 256

    rows_each = tokens // tp_count
    features = heads * HEAD_SIZE

    def kernel(
        q_ref, own_ref, gain_ref, all_ref, heads_ref,
        out_ref, top, norm, acc, z_send, x_send, recv, h_send, h_recv, sem,
    ):
        me, t = lax.axis_index("sp"), lax.axis_index("tp")
        z, x = me // width, me % width
        beside = z * width + (1 - x)
        barrier = pltpu.get_barrier_semaphore()
        peers = [lax.rem(z + step, planes) * width + x for step in range(1, planes)] + [beside]
        for peer in peers:
            pl.semaphore_signal(barrier, inc=1, device_id={"sp": peer}, device_id_type=MESH)
        for step in range(1, tp_count):
            pl.semaphore_signal(
                barrier,
                inc=1,
                device_id={"tp": lax.rem(t + step, tp_count)},
                device_id_type=MESH,
            )
        kept = pltpu.make_async_copy(own_ref, all_ref.at[me], sem)
        kept.start()
        pl.semaphore_wait(barrier, len(peers) + tp_count - 1)

        def along(step):
            return pltpu.make_async_remote_copy(
                src_ref=own_ref,
                dst_ref=all_ref.at[me],
                send_sem=z_send.at[step],
                recv_sem=recv.at[me],
                device_id={"sp": lax.rem(z + step, planes) * width + x},
                device_id_type=MESH,
            )

        def across(step, column):
            source = lax.rem(z + step, planes) * width + column
            return pltpu.make_async_remote_copy(
                src_ref=own_ref if step == 0 else all_ref.at[source],
                dst_ref=all_ref.at[source],
                send_sem=x_send.at[step],
                recv_sem=recv.at[source],
                device_id={"sp": beside},
                device_id_type=MESH,
            )

        across(0, x).start()
        for step in range(1, planes):
            along(step).start()
        kept.wait()

        def absorb(slot, first):
            keys = all_ref[slot, 0:tokens, 0:HEAD_SIZE]
            vals = all_ref[slot, 0:tokens, HEAD_SIZE : 2 * HEAD_SIZE]
            for start in range(0, span, chunk):
                part = pl.ds(start, chunk)
                scores = jnp.dot(keys, q_ref[:, part], preferred_element_type=jnp.float32)
                peak = jnp.max(scores, axis=0, keepdims=True)
                if not first:
                    old = top[:, part]
                    peak = jnp.maximum(old, peak)
                    factor = jnp.exp(old - peak)
                terms = jnp.exp(scores - peak)
                amount = jnp.sum(terms, axis=0, keepdims=True)
                mixed = lax.dot_general(
                    vals,
                    terms.astype(jnp.bfloat16),
                    (((0,), (0,)), ((), ())),
                    preferred_element_type=jnp.float32,
                )
                if not first:
                    amount = norm[:, part] * factor + amount
                    mixed = acc[:, part] * factor + mixed
                top[:, part] = peak
                norm[:, part] = amount
                acc[:, part] = mixed

        def block(step, column):
            return lax.rem(z + step, planes) * width + column

        absorb(me, True)
        for step in range(1, planes + 1):
            if step < planes:
                across(step, x).wait_recv()
                across(step, x).start()
            across(step - 1, 1 - x).wait_recv()
            absorb(block(step - 1, 1 - x), False)
            if step < planes:
                absorb(block(step, x), False)

        attended = acc[...] / norm[...]
        mean_sq = jnp.mean(attended * attended, axis=0, keepdims=True)
        rows = (attended * lax.rsqrt(mean_sq + EPS)).T
        for h in range(heads):
            out_ref[:, h * HEAD_SIZE : (h + 1) * HEAD_SIZE] = (
                rows[h * tokens : (h + 1) * tokens] * gain_ref[h : h + 1, :]
            ).astype(jnp.bfloat16)
        mine = heads_ref.at[:, pl.ds(pl.multiple_of(t * features, 128), features)]

        def part_of(peer):
            return out_ref.at[pl.ds(pl.multiple_of(peer * rows_each, 16), rows_each)]

        swaps = []
        for step in range(1, tp_count):
            peer = lax.rem(t + step, tp_count)
            swap = pltpu.make_async_remote_copy(
                src_ref=part_of(peer),
                dst_ref=mine,
                send_sem=h_send.at[step],
                recv_sem=h_recv.at[step],
                device_id={"tp": peer},
                device_id_type=MESH,
            )
            swap.start()
            swaps.append(swap)
        kept = pltpu.make_async_copy(part_of(t), mine, sem)
        kept.start()
        kept.wait()
        for swap in swaps:
            swap.wait()
        for step in range(planes):
            if step > 0:
                along(step).wait_send()
            across(step, x).wait_send()

    vmem = pl.BlockSpec(memory_space=pltpu.VMEM)
    dma = pltpu.SemaphoreType.DMA
    return pl.pallas_call(
        kernel,
        out_shape=(
            jax.ShapeDtypeStruct((count,) + own.shape, jnp.bfloat16),
            jax.ShapeDtypeStruct((rows_each, tp_count * features), jnp.bfloat16),
        ),
        in_specs=[vmem] * 3,
        out_specs=(vmem, vmem),
        scratch_shapes=[
            pltpu.VMEM((tokens, features), jnp.bfloat16),
            pltpu.VMEM((1, span), jnp.float32),
            pltpu.VMEM((1, span), jnp.float32),
            pltpu.VMEM((HEAD_SIZE, span), jnp.float32),
            dma((planes,)),
            dma((planes,)),
            dma((count,)),
            dma((tp_count,)),
            dma((tp_count,)),
            dma,
        ],
        compiler_params=pltpu.CompilerParams(collective_id=call_id, has_side_effects=True),
        name="attend",
    )(queries_t, own, gain)


def scan_attention(query_rows, key_blocks, score_scale):
    start_state = (
        jnp.full((query_rows.shape[0],), -1e30, jnp.float32),
        jnp.zeros((query_rows.shape[0],), jnp.float32),
        jnp.zeros(query_rows.shape, jnp.float32),
    )

    def step(carry, key_slab):
        run_max, run_total, run_acc = carry
        scores = (
            lax.dot_general(
                query_rows,
                key_slab[:, :HEAD_SIZE],
                (((1,), (1,)), ((), ())),
                preferred_element_type=jnp.float32,
            )
            * score_scale
        )
        new_max = jnp.maximum(run_max, jnp.max(scores, axis=1))
        factor = jnp.exp(run_max - new_max)
        expo_terms = jnp.exp(scores - new_max[:, None])
        new_total = run_total * factor + jnp.sum(expo_terms, axis=1)
        new_acc = run_acc * factor[:, None] + jnp.dot(
            expo_terms.astype(jnp.bfloat16),
            key_slab[:, HEAD_SIZE:],
            preferred_element_type=jnp.float32,
        )
        return ((new_max, new_total, new_acc), None)

    (_, run_total, run_acc), _ = lax.scan(step, start_state, key_blocks)
    return run_acc / run_total[:, None]


def across_pairs(shard, tp_count):
    return lax.ppermute(shard, "tp", [(i, i ^ 2) for i in range(tp_count)])


def slot_ranks(member):
    order = jnp.arange(member.shape[0], dtype=jnp.int32)
    before = (order[:, None] > order[None, :]).astype(jnp.bfloat16)
    rank = jnp.dot(before, member.astype(jnp.bfloat16), preferred_element_type=jnp.float32)
    return jnp.where(member, rank.astype(jnp.int32), -1)


def expert_block(flat_rows, gate_local, up_local, down_local):
    gate_out = jnp.dot(flat_rows, gate_local, preferred_element_type=jnp.float32)
    up_out = jnp.dot(flat_rows, up_local, preferred_element_type=jnp.float32)
    expert_inner = (jax.nn.silu(gate_out) * up_out).astype(jnp.bfloat16)
    return jnp.dot(expert_inner, down_local, preferred_element_type=jnp.float32).astype(
        jnp.bfloat16
    )


def local(
    queries,
    key_matrix,
    values,
    query_gain,
    key_norm_gain,
    head_gain,
    out_proj,
    residual,
    ffn_gain,
    routes,
    route_weights,
    expert_gate,
    expert_up,
    expert_down,
    shared_gate,
    shared_up,
    shared_down,
):
    tok_count = queries.shape[0]
    head_count = queries.shape[1] // HEAD_SIZE
    sp_count = lax.axis_size("sp")
    tp_count = lax.axis_size("tp")
    tp_index = lax.axis_index("tp")
    sequence_total = tok_count * sp_count
    positions = lax.axis_index("sp") * tok_count + jnp.arange(tok_count, dtype=jnp.int32)
    cosine_table, sine_table = grid_tables(positions, sequence_total)
    rotated_query = apply_rotary(
        final_norm(
            queries.astype(jnp.float32).reshape(tok_count, head_count, HEAD_SIZE), query_gain
        ),
        cosine_table,
        sine_table,
    ).astype(jnp.bfloat16)
    rotated_key = (
        apply_rotary(
            final_norm(
                key_matrix.astype(jnp.float32).reshape(tok_count, 1, HEAD_SIZE), key_norm_gain
            ),
            cosine_table,
            sine_table,
        )
        .reshape(tok_count, HEAD_SIZE)
        .astype(jnp.bfloat16)
    )
    packed = jnp.concatenate([rotated_key, values], axis=1)
    score_scale = HEAD_SIZE ** (-0.5)
    topk_count = routes.shape[1]
    capacity = max(2, 2 * tok_count * topk_count // (sp_count * tp_count))
    lanes = 2 * HEAD_SIZE
    entries = tok_count * topk_count
    relayed = (
        tp_count == 4
        and sp_count == 2 * tp_count
        and capacity % 16 == 0
        and tok_count % (16 * tp_count) == 0
        and entries % lanes == 0
        and head_count * tok_count % 256 == 0
        and head_count % 2 == 0
    )
    if relayed:
        shared_shards = []
        for shard in (shared_gate, shared_up, shared_down):
            shared_shards += [shard, across_pairs(shard, tp_count)]
        scale_hi = lax.reduce_precision(route_weights, 8, 7)
        tables = jnp.stack([routes.astype(jnp.float32), scale_hi, route_weights - scale_hi])
        tables = tables.astype(jnp.bfloat16).reshape(-1, lanes)
        table_rows = tables.shape[0]
        tables = jnp.pad(tables, ((0, -table_rows % 16), (0, 0)))
        scaled = rotated_query * jnp.asarray(score_scale, jnp.bfloat16)
        everything, token_heads = attend(
            scaled.transpose(2, 1, 0).reshape(HEAD_SIZE, head_count * tok_count),
            jnp.concatenate([packed, tables], axis=0),
            head_gain.reshape(head_count, HEAD_SIZE),
            tok_count,
            sp_count // tp_count,
            tp_count,
            0,
        )
        tables = everything[:, tok_count : tok_count + table_rows]
    else:
        piece = exchange(packed, "sp", 0, True).reshape(sequence_total, lanes)
        query_rows = rotated_query.transpose(1, 0, 2).reshape(head_count * tok_count, HEAD_SIZE)
        block_length = key_block_rows(sequence_total)
        key_blocks = piece.reshape(sequence_total // block_length, block_length, lanes)
        attended = scan_attention(query_rows, key_blocks, score_scale)
        attended = attended.reshape(head_count, tok_count, HEAD_SIZE).transpose(1, 0, 2)
        head_out = final_norm(attended, head_gain.reshape(head_count, HEAD_SIZE))
        head_out = head_out.astype(jnp.bfloat16).reshape(tok_count, head_count * HEAD_SIZE)
    part_rows = tok_count // tp_count
    if not relayed:
        token_heads = exchange(
            head_out.reshape(tp_count, part_rows, head_count * HEAD_SIZE), "tp", 1, False
        )
        token_heads = token_heads.transpose(1, 0, 2).reshape(part_rows, -1)
    own_resid = lax.dynamic_slice_in_dim(residual, tp_index * part_rows, part_rows, 0)
    hidden_own = (
        own_resid.astype(jnp.float32)
        + jnp.dot(token_heads, out_proj, preferred_element_type=jnp.float32)
    ).astype(jnp.bfloat16)
    normed_own = final_norm(hidden_own.astype(jnp.float32), ffn_gain).astype(jnp.bfloat16)
    model_width = normed_own.shape[1]
    gate_local = expert_gate[0]
    up_local = expert_up[0]
    down_local = expert_down[0]
    if relayed:
        width = sp_count // tp_count
        sp_index = lax.axis_index("sp")
        stood_for = proxy_plane(tp_index) * width + sp_index % width
        block_tables = lax.dynamic_index_in_dim(tables, stood_for, 0, keepdims=False)
        block_tables = block_tables.astype(jnp.float32).reshape(3, tok_count, topk_count)
        group = width * tp_count
        plane_experts = (sp_index // width) * group + jnp.arange(group, dtype=jnp.int32)
        named = block_tables[0].astype(jnp.int32)[:, :, None] == plane_experts[None, None, :]
        rank = slot_ranks(jnp.any(named, axis=1))
        slots = jnp.arange(capacity, dtype=jnp.int32)
        select = (rank.T[:, None, :] == slots[None, :, None]).astype(jnp.bfloat16)

        def combine(part):
            scale = jnp.sum(jnp.where(named, block_tables[part][:, :, None], 0.0), axis=1)
            table = select * scale.T.astype(jnp.bfloat16)[:, None, :]
            return table.reshape(group * capacity, tok_count)

        combine_hi, combine_lo = combine(1), combine(2)
        arrived, *others = dispatch(
            normed_own, select, shared_shards, tp_count, width, tp_count, 2
        )
        produced = expert_block(
            arrived.reshape(sp_count * capacity, model_width), gate_local, up_local, down_local
        )
        every_shard = []
        for i in range(0, len(shared_shards), 2):
            every_shard += shared_shards[i : i + 2] + others[i : i + 2]
        routed, shared_out = give_back(
            produced.reshape(sp_count, capacity, model_width),
            combine_hi,
            combine_lo,
            normed_own,
            every_shard,
            tp_count,
            width,
            tp_count,
            3,
        )
        return (
            hidden_own.astype(jnp.float32) + (shared_out + routed.astype(jnp.float32))
        ).astype(jnp.bfloat16)
    normed = exchange(normed_own, "tp", 2, True).reshape(tok_count, model_width)
    slot_total = sp_count * capacity
    experts_here = jnp.arange(sp_count, dtype=jnp.int32) * tp_count + tp_index
    named = routes[:, :, None] == experts_here[None, None, :]
    member = jnp.any(named, axis=1)
    scale = jnp.sum(jnp.where(named, route_weights[:, :, None], 0.0), axis=1)
    rank = slot_ranks(member)
    slots = jnp.arange(capacity, dtype=jnp.int32)
    chosen = rank.T[:, None, :] == slots[None, :, None]
    select = chosen.astype(jnp.bfloat16).reshape(slot_total, tok_count)
    outgoing = jnp.dot(select, normed, preferred_element_type=jnp.float32).astype(jnp.bfloat16)
    arrived = exchange(outgoing.reshape(sp_count, capacity, model_width), "sp", 3, False)
    produced = expert_block(
        arrived.reshape(slot_total, model_width), gate_local, up_local, down_local
    )
    returned = exchange(produced.reshape(sp_count, capacity, model_width), "sp", 4, False).reshape(
        slot_total, model_width
    )
    combine = jnp.where(chosen, scale.T[:, None, :], 0.0).reshape(slot_total, tok_count)
    combine_hi = lax.reduce_precision(combine, 8, 7)
    combine_lo = (combine - combine_hi).astype(jnp.bfloat16)
    combine_hi = combine_hi.astype(jnp.bfloat16)

    def mix(weights):
        return lax.dot_general(
            weights, returned, (((0,), (0,)), ((), ())), preferred_element_type=jnp.float32
        )

    gate_part = jnp.dot(normed, shared_gate, preferred_element_type=jnp.float32)
    up_part = jnp.dot(normed, shared_up, preferred_element_type=jnp.float32)
    shared_inner = (jax.nn.silu(gate_part) * up_part).astype(jnp.bfloat16)
    shares = (
        jnp.dot(shared_inner, shared_down, preferred_element_type=jnp.float32)
        + mix(combine_hi)
        + mix(combine_lo)
    ).astype(jnp.bfloat16)
    shares = exchange(shares.reshape(tp_count, part_rows, model_width), "tp", 5, False)
    mixed_rows = jnp.sum(shares.astype(jnp.float32), axis=0)
    return (hidden_own.astype(jnp.float32) + mixed_rows).astype(jnp.bfloat16)


def solution(mesh):
    placed = (
        P("sp", "tp"),
        P("sp", "tp"),
        P("sp", "tp"),
        P(),
        P(),
        P("tp"),
        P(),
        P("sp", None),
        P(),
        P("sp", None),
        P("sp", None),
        P(("sp", "tp"), None, None),
        P(("sp", "tp"), None, None),
        P(("sp", "tp"), None, None),
        P(None, "tp"),
        P(None, "tp"),
        P("tp", None),
    )
    return jax.shard_map(
        local, mesh=mesh, in_specs=placed, out_specs=P(("sp", "tp"), None), check_vma=False
    )
```

profile of v0, /device:TPU:0, one launch (start us, length us, event | category | flops | bytes accessed | tf_op | source)
XLA Modules:
  0.0 190.5 jit_solution(2703454892424372757)
XLA Ops:
  0.0 3.1 %collective-permute-start = (bf16[2048,128]{1,0:T(8,128)(2,1)}, bf16[2048,128]{1,0:T(8,128)(2,1)S(1)}, u32[]{:S(2)}, u32[]{:S(2)}) collective-permute-start(bf16[2048,128]{1,0:T(8,128)(2,1)} %refs_0_.3), channel_id=1, source_target_pairs={{0,2},{1,3},{2,0},{3,1},{4,6},{5,7},{6,4},{7,5},{8,10},{9,11},{10,... | collective-permute-start | bytes 1572872 | tf_op jit(solution)/shard_map/ppermute | solution.py:692
  3.2 1.9 %collective-permute-start.2 = (bf16[128,2048]{1,0:T(8,128)(2,1)}, bf16[128,2048]{1,0:T(8,128)(2,1)}, u32[]{:S(2)}, u32[]{:S(2)}) collective-permute-start(bf16[128,2048]{1,0:T(8,128)(2,1)} %refs_8_.1), channel_id=1, source_target_pairs={{0,2},{1,3},{2,0},{3,1},{4,6},{5,7},{6,4},{7,5},{8,10},{9,11},{10,... | collective-permute-start | bytes 1572872 | tf_op jit(solution)/shard_map/ppermute | solution.py:692
  5.1 0.7 mul.242
  5.9 1.1 copy.29
  7.2 0.2 fusion.25
  7.3 0.1 multiply_multiply_fusion
  7.6 0.2 copy.38
  7.7 0.8 reshape.409.q_ref
  8.6 0.2 copy.33
  8.8 0.3 convert_element_type.104
  9.2 0.1 copy.32
  9.4 0.2 subtract_convert_fusion.1
  9.7 0.1 copy.31
  9.8 0.7 reshape.411.gain_ref
  10.5 0.7 fusion.19.own_ref
  11.2 29.0 %attend.1 = (bf16[8,352,128]{2,1,0:T(8,128)(2,1)}, bf16[80,1024]{1,0:T(8,128)(2,1)}) custom-call(bf16[64,1280]{1,0:T(8,128)(2,1)} %reshape.409.q_ref, bf16[352,128]{1,0:T(8,128)(2,1)} %fusion.19.own_ref, f32[4,64]{1,0:T(4,128)} %reshape.411.gain_ref), custom_call_target="tpu_custom_call" | custom-call | tf_op jit(solution)/shard_map/attend/pallas_call | solution.py:633
  40.2 3.3 %multiply_reduce_fusion = (f32[80]{0:T(128)S(1)}, f32[80,2048]{1,0:T(8,128)S(1)}) fusion(bf16[80,1024]{1,0:T(8,128)(2,1)} %get-tuple-element.16, bf16[1024,2048]{1,0:T(8,128)(2,1)} %param.23, bf16[320,2048]{1,0:T(8,128)(2,1)} %param.24, s32[]{:T(128)S(6)} %select_n.56), kind=kOutput, calls=%fused_computation.20 | convolution fusion | flops 336527296 | bytes 5341508 | tf_op jit(solution)/shard_map/dot_general | solution.py:809
  43.5 0.8 slice.34
  44.4 0.2 convert_element_type.110
  44.7 0.1 fusion.7
  44.8 1.0 fusion.10.sel_ref
  45.8 0.2 broadcast_in_dim.30
  46.1 0.2 broadcast_in_dim.23
  46.4 0.1 fusion.21
  46.6 1.2 fusion.8
  47.8 0.8 multiply_convert_fusion.2.own_ref
  48.7 0.8 copy-done.1
  49.4 55.7 %dispatch.1 = (bf16[8,80,2048]{2,1,0:T(8,128)(2,1)}, bf16[2048,128]{1,0:T(8,128)(2,1)}, bf16[2048,128]{1,0:T(8,128)(2,1)}, bf16[2048,128]{1,0:T(8,128)(2,1)}, bf...) custom-call(bf16[80,2048]{1,0:T(8,128)(2,1)} %multiply_convert_fusion.2.own_ref, ...), custom_call_target="tpu_custom_call" | custom-call | tf_op jit(solution)/shard_map/dispatch/pallas_call | solution.py:290
  105.1 5.0 %fusion.3 = f32[640,512]{1,0:T(8,128)} fusion(bf16[640,2048]{1,0:T(8,128)(2,1)} %bitcast.70, bf16[1,2048,512]{2,1,0:T(8,128)(2,1)} %param.29), kind=kOutput, calls=%fused_computation.5 | convolution fusion | flops 1342177280 | bytes 6029312 | tf_op jit(solution)/shard_map/dot_general | solution.py:704
  110.1 7.3 %convolution_convert_fusion = bf16[640,2048]{1,0:T(8,128)(2,1)} fusion(bf16[1,512,2048]{2,1,0:T(8,128)(2,1)S(1)} %copy-done, f32[640,512]{1,0:T(8,128)} %fusion.3, bf16[640,2048]{1,0:T(8,128)(2,1)} %bitcast.71, bf16[1,2048,512]{2,1,0:T(8,128)(2,1)} %param.28), kind=kOutput, calls=%fused_computation | convolution fusion | flops 2687631360 | bytes 10747904 | tf_op jit(solution)/shard_map/dot_general | solution.py:706
  117.4 71.1 %give_back.1 = (bf16[80,2048]{1,0:T(8,128)(2,1)}, f32[80,2048]{1,0:T(8,128)}) custom-call(bf16[8,80,2048]{2,1,0:T(8,128)(2,1)} %bitcast.60, bf16[640,320]{1,0:T(8,128)(2,1)} %get-tuple-element.36.hi_ref, bf16[640,320]{1,0:T(8,128)(2,1)} %get-tuple-element.35.lo_ref, bf16[80,2048]{1,0:T(8,128)(2,1)} %multiply_convert_fusion.2.own_ref, ...), custom_call_target="tpu_custom_call" | custom-call | tf_op jit(solution)/shard_map/give_back/pallas_call | solution.py:472
  188.5 2.0 %add_convert_fusion = bf16[80,2048]{1,0:T(8,128)(2,1)} fusion(f32[80,2048]{1,0:T(8,128)S(1)} %get-tuple-element.49, f32[80,2048]{1,0:T(8,128)} %get-tuple-element.25, bf16[80,2048]{1,0:T(8,128)(2,1)} %get-tuple-element.26), kind=kLoop, calls=%fused_computation.17 | loop fusion | flops 655360 | bytes 1966080 | tf_op jit(solution)/shard_map/convert_element_type | solution.py:857
  (45 shorter events, 1.0 us)
Async XLA Ops:
  0.0 110.1 %copy-start = (bf16[1,512,2048]{2,1,0:T(8,128)(2,1)S(1)}, bf16[1,512,2048]{2,1,0:T(8,128)(2,1)}, u32[]{:S(2)}) copy-start(bf16[1,512,2048]{2,1,0:T(8,128)(2,1)} %param.30) | copy-start | bytes 6291460
  0.0 8.6 %copy-start.5 = (f32[320,4]{0,1:T(4,128)S(1)}, f32[320,4]{0,1:T(4,128)}, u32[]{:S(2)}) copy-start(f32[320,4]{0,1:T(4,128)} %param.27) | copy-start | bytes 15364
  0.0 8.6 %copy-start.6 = (s32[320,4]{0,1:T(4,128)S(1)}, s32[320,4]{0,1:T(4,128)}, u32[]{:S(2)}) copy-start(s32[320,4]{0,1:T(4,128)} %param.26) | copy-start | bytes 15364
  0.0 9.2 %copy-start.3 = (bf16[320,64]{0,1:T(8,128)(2,1)S(1)}, bf16[320,64]{0,1:T(8,128)(2,1)}, u32[]{:S(2)}) copy-start(bf16[320,64]{0,1:T(8,128)(2,1)} %param.19) | copy-start | bytes 122884
  0.0 9.3 %copy-start.2 = (bf16[320,64]{0,1:T(8,128)(2,1)S(1)}, bf16[320,64]{0,1:T(8,128)(2,1)}, u32[]{:S(2)}) copy-start(bf16[320,64]{0,1:T(8,128)(2,1)} %param.18) | copy-start | bytes 122884
  0.0 9.3 %copy-start.8 = (f32[64]{0:T(128)S(1)}, f32[64]{0:T(128)}, u32[]{:S(2)}) copy-start(f32[64]{0:T(128)} %param.21) | copy-start | bytes 772
  0.0 48.6 %collective-permute-start = (bf16[2048,128]{1,0:T(8,128)(2,1)}, bf16[2048,128]{1,0:T(8,128)(2,1)S(1)}, u32[]{:S(2)}, u32[]{:S(2)}) collective-permute-start(bf16[2048,128]{1,0:T(8,128)(2,1)} %refs_0_.3), channel_id=1, source_target_pairs={{0,2},{1,3},{2,0},{3,1},{4,6},{5,7},{6,4},{7,5},{8,10},{9,11},{10,... | collective-permute-start | bytes 1572872 | tf_op jit(solution)/shard_map/ppermute | solution.py:692
  3.1 45.5 %collective-permute-start.1 = (bf16[2048,128]{1,0:T(8,128)(2,1)}, bf16[2048,128]{1,0:T(8,128)(2,1)}, u32[]{:S(2)}, u32[]{:S(2)}) collective-permute-start(bf16[2048,128]{1,0:T(8,128)(2,1)} %refs_4_.3), channel_id=1, source_target_pairs={{0,2},{1,3},{2,0},{3,1},{4,6},{5,7},{6,4},{7,5},{8,10},{9,11},{10,... | collective-permute-start | bytes 1572872 | tf_op jit(solution)/shard_map/ppermute | solution.py:692
  3.2 45.5 %collective-permute-start.2 = (bf16[128,2048]{1,0:T(8,128)(2,1)}, bf16[128,2048]{1,0:T(8,128)(2,1)}, u32[]{:S(2)}, u32[]{:S(2)}) collective-permute-start(bf16[128,2048]{1,0:T(8,128)(2,1)} %refs_8_.1), channel_id=1, source_target_pairs={{0,2},{1,3},{2,0},{3,1},{4,6},{5,7},{6,4},{7,5},{8,10},{9,11},{10,... | collective-permute-start | bytes 1572872 | tf_op jit(solution)/shard_map/ppermute | solution.py:692
  7.0 2.8 %copy-start.7 = (f32[256]{0:T(256)S(1)}, f32[256]{0:T(256)}, u32[]{:S(2)}) copy-start(f32[256]{0:T(256)} %param.22) | copy-start | bytes 3076
  43.5 4.3 %copy-start.4 = (f32[2048]{0:T(1024)S(1)}, f32[2048]{0:T(1024)}, u32[]{:S(2)}) copy-start(f32[2048]{0:T(1024)} %param.25) | copy-start | bytes 24580
  48.6 0.8 copy-start.1
where the time goes:
time: 194 us; the launch traced here: 191 us
  Pallas kernels  156 us (80%)
  matrix products  15.7 us (8%)
  other arithmetic  6.89 us (4%)
  local copies, waits for them, and re-layouts  6.77 us (3%)
  starting transfers between devices  5.09 us (3%)
    pallas_call x1, Pallas kernels, give_back(): pl.pallas_call(kernel, out_shape=(jax.ShapeDtypeStruct((rows, model), jnp...  71.1 us
    pallas_call x1, Pallas kernels, dispatch(): pl.pallas_call(kernel, out_shape=[jax.ShapeDtypeStruct((planes * width, c...  55.7 us
    pallas_call x1, Pallas kernels, attend(): pl.pallas_call(kernel, out_shape=(jax.ShapeDtypeStruct((count,) + own.sha...  29 us
    dot_general x1, matrix products, expert_block(): jnp.dot(expert_inner, down_local, preferred_element_type=jnp.float32)  7.28 us
    ppermute x3, starting transfers between devices, across_pairs(): return lax.ppermute(shard, 'tp', [(i, i ^ 2) for i in range(tp_count)])  5.09 us
    dot_general x1, matrix products, expert_block(): up_out = jnp.dot(flat_rows, up_local, preferred_element_type=jnp.float32)  5 us
  transfers between devices with their start and end apart: 3, of which 0 were waited for; matrix products, arithmetic and copies ran while one was open for 7% of the time, Pallas kernels for 15%

commit v1 on v0

v1 whole, which is shorter than its diff:
```python
import jax
import jax.numpy as jnp
from jax import lax
from jax.experimental import pallas as pl
from jax.experimental.pallas import tpu as pltpu
from jax.sharding import PartitionSpec as P

HEAD_SIZE = 64
GRID_W = 64


EPS = 1e-06
THETA = 10000.0


def final_norm(field, gain):
    mean_sq = jnp.mean(field * field, axis=-1, keepdims=True)
    return field * lax.rsqrt(mean_sq + EPS) * gain


def grid_tables(positions, sequence_total):
    grid_rows = sequence_total // GRID_W
    row_pos = (positions // GRID_W - grid_rows // 2).astype(jnp.float32)
    col_pos = (positions % GRID_W - GRID_W // 2).astype(jnp.float32)
    quarter = HEAD_SIZE // 4
    inverse = THETA ** (-jnp.arange(quarter, dtype=jnp.float32) / quarter)
    angles = jnp.concatenate([row_pos[:, None] * inverse, col_pos[:, None] * inverse], axis=1)
    return (jnp.cos(angles), jnp.sin(angles))


def apply_rotary(field, cosine_table, sine_table):
    row_count, head_count = (field.shape[0], field.shape[1])
    quarter = HEAD_SIZE // 4
    pieces = field.reshape(row_count, head_count, 2, 2, quarter)
    front_half = pieces[:, :, :, 0, :].reshape(row_count, head_count, 2 * quarter)
    back_half = pieces[:, :, :, 1, :].reshape(row_count, head_count, 2 * quarter)
    cos_wide = cosine_table[:, None, :]
    sin_wide = sine_table[:, None, :]
    new_front = (front_half * cos_wide - back_half * sin_wide).reshape(
        row_count, head_count, 2, 1, quarter
    )
    new_back = (front_half * sin_wide + back_half * cos_wide).reshape(
        row_count, head_count, 2, 1, quarter
    )
    return jnp.concatenate([new_front, new_back], axis=3).reshape(row_count, head_count, HEAD_SIZE)


def exchange(block, axis, call_id, gather):
    count = lax.axis_size(axis)
    if count == 1:
        return block[None] if gather else block
    shape = (count,) + block.shape if gather else block.shape

    def kernel(in_ref, out_ref, send_sems, recv_sems, own_sem):
        me = lax.axis_index(axis)
        barrier = pltpu.get_barrier_semaphore()
        for step in range(1, count):
            pl.semaphore_signal(
                barrier,
                inc=1,
                device_id={axis: lax.rem(me + step, count)},
                device_id_type=pl.DeviceIdType.MESH,
            )
        own = pltpu.make_async_copy(in_ref if gather else in_ref.at[me], out_ref.at[me], own_sem)
        own.start()
        pl.semaphore_wait(barrier, count - 1)
        copies = []
        for step in range(1, count):
            peer = lax.rem(me + step, count)
            copy = pltpu.make_async_remote_copy(
                src_ref=in_ref if gather else in_ref.at[peer],
                dst_ref=out_ref.at[me],
                send_sem=send_sems.at[step],
                recv_sem=recv_sems.at[step],
                device_id={axis: peer},
                device_id_type=pl.DeviceIdType.MESH,
            )
            copy.start()
            copies.append(copy)
        own.wait()
        for copy in copies:
            copy.wait()

    return pl.pallas_call(
        kernel,
        out_shape=jax.ShapeDtypeStruct(shape, block.dtype),
        in_specs=[pl.BlockSpec(memory_space=pltpu.VMEM)],
        out_specs=pl.BlockSpec(memory_space=pltpu.VMEM),
        scratch_shapes=[
            pltpu.SemaphoreType.DMA((count,)),
            pltpu.SemaphoreType.DMA((count,)),
            pltpu.SemaphoreType.DMA,
        ],
        compiler_params=pltpu.CompilerParams(collective_id=call_id, has_side_effects=True),
        name="exchange_%d" % call_id,
    )(block)


def key_block_rows(piece_rows):
    return max((width for width in range(1, 2049) if piece_rows % width == 0))


MESH = pl.DeviceIdType.MESH
COLUMNS = 512
FLIPS = ((1, 2), (1, 3), (0, 2), (0, 3), (1, 0), (1, 1), (0, 1))
TP_FLIPS = (2, 3, 1)


def remote(source, target, send_sem, recv_sem, device):
    return pltpu.make_async_remote_copy(
        src_ref=source,
        dst_ref=target,
        send_sem=send_sem,
        recv_sem=recv_sem,
        device_id=device,
        device_id_type=MESH,
    )


def whole_layer(
    queries_t,
    packet,
    gain,
    ffn_gain,
    residual,
    weights,
    tokens,
    capacity,
    topk,
    width,
    tp_count,
    call_id,
):
    count = lax.axis_size("sp")
    planes = count // width
    group = width * tp_count
    span = queries_t.shape[1]
    heads = gain.shape[0]
    features = heads * HEAD_SIZE
    model = residual.shape[1]
    quarter = model // tp_count
    rows_each = tokens // tp_count
    chunk = 256
    lane_groups = -(-tokens // 128)
    lanes = 128 * lane_groups
    table_rows = packet.shape[0] - tokens
    table_step = table_rows // lane_groups
    slots = group * capacity
    out_proj, gate_w, up_w, down_w, shared_gate, shared_up, shared_down = weights
    hidden_units = gate_w.shape[1]
    shared_units = shared_gate.shape[1]
    pair = width * capacity
    half = tokens // 2
    bf16, f32 = jnp.bfloat16, jnp.float32

    def kernel(
        q_ref, own_ref, gain_ref, ffn_ref, resid_ref, wo_hbm, wg_hbm, wu_hbm, wd_hbm,
        sg_hbm, su_hbm, sd_hbm, out_ref,
        kv, top, norm, acc, tri, ranks, scales, sel, sel_t, rblk, hblk, rpack, hpack,
        xr, xh, hs, ns, ret, rr, passed, arrived, base, fin, hg, own_hid, si, sdq,
        res, wo, wg, wu, wd, sg, su,
        w_sem, k_sem, kz_send, kx_send, k_recv,
        rz_send, rz_recv, ri_send, ri_recv, hz_send, hz_recv, hi_send, hi_recv,
        hg_send, hg_recv, sd_send, sd_recv, si_send, si_recv,
        rt_send, rt_recv, zr_send, zr_recv, f_send, f_recv,
    ):
        me, t = lax.axis_index("sp"), lax.axis_index("tp")
        z, x = me // width, me % width
        p = x * tp_count + t
        side = z // 2
        inner = jnp.where((z == 1) | (z == 2), 1, 0)

        def nearest(k):
            near = k + inner * (1 - 2 * k) if k < 2 else k
            return near + side * (planes - 1 - 2 * near)

        def mate(dx, dt):
            x2 = 1 - x if dx else x
            t2 = t
            if dt & 2:
                t2 = t2 + 2 * (1 - 2 * (t // 2))
            if dt & 1:
                t2 = t2 + (1 - 2 * (t % 2))
            return x2, t2

        def at(plane, x2, t2):
            return {"sp": plane * width + x2, "tp": t2}

        arrived[...] = jnp.zeros(arrived.shape, bf16)
        barrier = pltpu.get_barrier_semaphore()
        for dx, dt in FLIPS:
            pl.semaphore_signal(barrier, inc=1, device_id=at(z, *mate(dx, dt)), device_id_type=MESH)
        for step in range(1, planes):
            pl.semaphore_signal(
                barrier, inc=1, device_id=at(lax.rem(z + step, planes), x, t), device_id_type=MESH
            )

        def columns(index, size):
            return pl.ds(pl.multiple_of(index * size, 128), size)

        kept = pltpu.make_async_copy(own_ref, kv.at[me], k_sem.at[0])
        kept.start()
        mine = pltpu.make_async_copy(resid_ref.at[:, columns(t, quarter)], rblk.at[z], k_sem.at[1])
        mine.start()
        loads = [
            pltpu.make_async_copy(source, target, w_sem.at[i])
            for i, (source, target) in enumerate(
                [
                    (wo_hbm, wo), (wg_hbm, wg), (wu_hbm, wu), (wd_hbm, wd),
                    (sg_hbm, sg), (su_hbm, su), (resid_ref, res),
                ]
            )
        ]
        for load in loads:
            load.start()
        before = lax.broadcasted_iota(jnp.int32, (lanes, lanes), 0)
        after = lax.broadcasted_iota(jnp.int32, (lanes, lanes), 1)
        tri[...] = jnp.where(before < after, 1.0, 0.0).astype(bf16)
        top[...] = jnp.full(top.shape, -1e30, f32)
        norm[...] = jnp.zeros(norm.shape, f32)
        acc[...] = jnp.zeros(acc.shape, f32)
        kept.wait()
        mine.wait()
        pl.semaphore_wait(barrier, len(FLIPS) + planes - 1)

        def along(step):
            return remote(
                own_ref, kv.at[me], kz_send.at[step], k_recv.at[me],
                at(lax.rem(z + step, planes), x, t),
            )

        def came(slot):
            return remote(own_ref, kv.at[slot], kz_send.at[0], k_recv.at[slot], at(z, 1 - x, t))

        def across(plane):
            slot = plane * width + x
            return remote(kv.at[slot], kv.at[slot], kx_send.at[plane], k_recv.at[slot], at(z, 1 - x, t))

        def z_hop(blk, b, up, ssem, rsem):
            return remote(
                blk.at[b], blk.at[b], ssem.at[up, b], rsem.at[b],
                at(z + (1 if up else -1), x, t),
            )

        def goes(b, up):
            return (b <= z) & (z < planes - 1) if up else (b >= z) & (z > 0)

        def forward(blk, b, ssem, rsem):
            for up in (1, 0):
                @pl.when(goes(b, up))
                def _():
                    z_hop(blk, b, up, ssem, rsem).start()

        def landed(b, wide, dst, x2, t2):
            return dst.at[b * width + x2, :, columns(t2, wide)]

        def deal_copy(b, pack, dst, wide, ssem, rsem, i):
            x2, t2 = mate(*FLIPS[i])
            rows = pl.ds(pl.multiple_of((x2 * tp_count + t2) * capacity, 16), capacity)
            return remote(
                pack.at[b, rows], landed(b, wide, dst, x, t), ssem.at[b, i], rsem.at[b, i],
                at(z, x2, t2),
            )

        def deal_own(b, pack, dst, wide, rsem):
            rows = pl.ds(pl.multiple_of(p * capacity, 16), capacity)
            return pltpu.make_async_copy(
                pack.at[b, rows], landed(b, wide, dst, x, t), rsem.at[b, len(FLIPS)]
            )

        def deal(b, blk, pack, dst, wide, ssem, rsem):
            for start in range(0, slots, tokens):
                pack[b, start : start + tokens, :] = jnp.dot(
                    sel[b, start : start + tokens, 0:tokens], blk[b], preferred_element_type=f32
                ).astype(bf16)
            for i in range(len(FLIPS)):
                deal_copy(b, pack, dst, wide, ssem, rsem, i).start()
            deal_own(b, pack, dst, wide, rsem).start()

        def dealt(b, pack, dst, wide, ssem, rsem):
            for i in range(len(FLIPS)):
                x2, t2 = mate(*FLIPS[i])
                remote(
                    pack.at[b, 0:capacity], landed(b, wide, dst, x2, t2), ssem.at[b, i],
                    rsem.at[b, i], at(z, x2, t2),
                ).wait_recv()
            deal_own(b, pack, dst, wide, rsem).wait()

        resid_path = (rblk, rpack, xr, quarter, ri_send, ri_recv)
        heads_path = (hblk, hpack, xh, features, hi_send, hi_recv)

        def table(slot):
            return kv[slot, tokens : tokens + table_rows, :].astype(f32)

        def index(b):
            rows = table(b * width + x)
            named = (lax.broadcasted_iota(jnp.int32, (group, 128), 0) + z * group).astype(f32)
            for j in range(lane_groups):
                hit = jnp.zeros((group, 128), f32)
                for k in range(topk):
                    row = rows[j * table_step + k : j * table_step + k + 1]
                    hit = jnp.where(row == named, 1.0, hit)
                ranks[0:group, 128 * j : 128 * j + 128] = hit
            member = ranks[0:group, :]
            rank = jnp.dot(member.astype(bf16), tri[...], preferred_element_type=f32)
            ranks[0:group, :] = jnp.where(member > 0.5, rank, -1.0)
            wanted = lax.broadcasted_iota(jnp.int32, (capacity, 128), 0).astype(f32)
            for e in range(group):
                for j in range(lane_groups):
                    row = ranks[e : e + 1, 128 * j : 128 * j + 128]
                    sel[b, e * capacity : (e + 1) * capacity, 128 * j : 128 * j + 128] = jnp.where(
                        row == wanted, 1.0, 0.0
                    ).astype(bf16)

        def weigh(slot, carry):
            rows = table(slot)
            mine_is = (z * group + p).astype(f32)
            amounts = []
            for j in range(lane_groups):
                hit = jnp.zeros((1, 128), f32)
                amount = jnp.zeros((1, 128), f32)
                for k in range(topk):
                    at_row = j * table_step + k
                    same = rows[at_row : at_row + 1] == mine_is
                    high = rows[at_row + topk : at_row + topk + 1]
                    low = rows[at_row + 2 * topk : at_row + 2 * topk + 1]
                    hit = jnp.where(same, 1.0, hit)
                    amount = jnp.where(same, high + low, amount)
                ranks[0:8, 128 * j : 128 * j + 128] = jnp.broadcast_to(hit, (8, 128))
                amounts.append(amount)
            member = ranks[0:8, :]
            rank = jnp.dot(member.astype(bf16), tri[...], preferred_element_type=f32)
            ranks[0:8, :] = jnp.where(member > 0.5, rank, -1.0)
            wanted = lax.broadcasted_iota(jnp.int32, (capacity, 128), 0).astype(f32)
            summed = jnp.zeros((capacity, 128), f32)
            for j in range(lane_groups):
                row = ranks[0:1, 128 * j : 128 * j + 128]
                summed = summed + jnp.where(row == wanted, amounts[j], 0.0)
            scales[slot] = jnp.broadcast_to(
                jnp.sum(summed, axis=1, keepdims=True), (capacity, 128)
            )
            return carry

        def absorb(slot):
            keys = kv[slot, 0:tokens, 0:HEAD_SIZE]
            vals_t = kv[slot, 0:tokens, HEAD_SIZE : 2 * HEAD_SIZE].T
            for start in range(0, span, chunk):
                part = pl.ds(start, chunk)
                scores = jnp.dot(keys, q_ref[:, part], preferred_element_type=f32)
                old = top[:, part]
                peak = jnp.maximum(old, jnp.max(scores, axis=0, keepdims=True))
                factor = jnp.exp(old - peak)
                terms = jnp.exp(scores - peak)
                norm[:, part] = norm[:, part] * factor + jnp.sum(terms, axis=0, keepdims=True)
                acc[:, part] = acc[:, part] * factor + jnp.dot(
                    vals_t, terms.astype(bf16), preferred_element_type=f32
                )
                top[:, part] = peak

        for step in range(1, planes):
            along(step).start()
        across(z).start()
        forward(rblk, z, rz_send, rz_recv)
        sd_copies = []
        for i, dt in enumerate(TP_FLIPS):
            _, t2 = mate(0, dt)
            copy = remote(
                sd_hbm.at[:, columns(t2, quarter)],
                sdq.at[pl.ds(pl.multiple_of(t * shared_units, 16), shared_units)],
                sd_send.at[i], sd_recv.at[i], at(z, x, t2),
            )
            sd_copies.append(copy)
        sd_own = pltpu.make_async_copy(
            sd_hbm.at[:, columns(t, quarter)],
            sdq.at[pl.ds(pl.multiple_of(t * shared_units, 16), shared_units)],
            sd_recv.at[len(TP_FLIPS)],
        )
        sd_own.start()
        index(z)
        deal(z, *resid_path)
        absorb(me)
        for k in range(1, planes):
            b, last = nearest(k), nearest(k - 1)
            came(b * width + x).wait_recv()
            across(b).start()
            index(b)
            z_hop(rblk, b, 0, rz_send, rz_recv).wait_recv()
            forward(rblk, b, rz_send, rz_recv)
            deal(b, *resid_path)
            came(last * width + (1 - x)).wait_recv()
            absorb(last * width + (1 - x))
            absorb(b * width + x)
        for copy in sd_copies:
            copy.start()
        last = nearest(planes - 1)
        came(last * width + (1 - x)).wait_recv()
        absorb(last * width + (1 - x))

        attended = acc[...] / norm[...]
        mean_sq = jnp.mean(attended * attended, axis=0, keepdims=True)
        rows = (attended * lax.rsqrt(mean_sq + EPS)).T
        for h in range(heads):
            hblk[z, :, h * HEAD_SIZE : (h + 1) * HEAD_SIZE] = (
                rows[h * tokens : (h + 1) * tokens] * gain_ref[h : h + 1, :]
            ).astype(bf16)

        forward(hblk, z, hz_send, hz_recv)
        deal(z, *heads_path)

        def gather(i):
            _, t2 = mate(0, TP_FLIPS[i])
            return remote(
                hblk.at[z], hg.at[:, columns(t, features)], hg_send.at[i], hg_recv.at[i],
                at(z, x, t2),
            )

        for i in range(len(TP_FLIPS)):
            gather(i).start()
        hg_own = pltpu.make_async_copy(
            hblk.at[z], hg.at[:, columns(t, features)], hg_recv.at[len(TP_FLIPS)]
        )
        hg_own.start()

        def pass_heads(k):
            b = nearest(k)
            z_hop(hblk, b, 0, hz_send, hz_recv).wait_recv()
            forward(hblk, b, hz_send, hz_recv)
            deal(b, *heads_path)

        def normalize(head_rows, resid_at):
            count_rows = head_rows.shape[0]
            squares = jnp.zeros((count_rows, 1), f32)
            for start in range(0, model, COLUMNS):
                part = slice(start, start + COLUMNS)
                field = jnp.dot(head_rows, wo[:, part], preferred_element_type=f32)
                field = (resid_at(part).astype(f32) + field).astype(bf16)
                hs[:, part] = field
                field = field.astype(f32)
                squares = squares + jnp.sum(field * field, axis=1, keepdims=True)
            inverse = lax.rsqrt(squares / model + EPS)
            for start in range(0, model, COLUMNS):
                part = slice(start, start + COLUMNS)
                ns[:, part] = (hs[:, part].astype(f32) * inverse * ffn_ref[:, part]).astype(bf16)

        def glu(gate_ref, up_ref):
            gate = jnp.dot(ns[...], gate_ref[...], preferred_element_type=f32)
            up = jnp.dot(ns[...], up_ref[...], preferred_element_type=f32)
            return (gate / (1.0 + jnp.exp(-gate)) * up).astype(bf16)

        def back_copy(b, j, i):
            x2, t2 = mate(*FLIPS[i])
            return remote(
                ret.at[b * width + x2, :, columns(t2, quarter)], rr.at[b, p],
                rt_send.at[b, i], rt_recv.at[b, i], at(z, x2, t2),
            )

        def back_own(b):
            return pltpu.make_async_copy(
                ret.at[b * width + x, :, columns(t, quarter)], rr.at[b, p],
                rt_recv.at[b, len(FLIPS)],
            )

        def expert(k):
            b = nearest(k)
            dealt(b, *resid_path[1:])
            dealt(b, *heads_path[1:])
            both = pl.ds(b * width, width)

            def resid_at(part):
                return xr[both, :, part].reshape(pair, COLUMNS)

            normalize(xh[both].reshape(pair, tp_count * features), resid_at)
            inner_rows = glu(wg, wu)
            scale = scales[both].reshape(pair, 128)[:, 0:1]
            for start in range(0, model, COLUMNS):
                part = slice(start, start + COLUMNS)
                made = jnp.dot(inner_rows, wd[:, part], preferred_element_type=f32) * scale
                ret[both, :, part] = made.astype(bf16).reshape(width, capacity, COLUMNS)
            for i in range(len(FLIPS)):
                back_copy(b, 0, i).start()
            back_own(b).start()

        def inner_copy(i):
            _, t2 = mate(0, TP_FLIPS[i])
            return remote(
                si.at[:, columns(t, shared_units)], si.at[:, columns(t, shared_units)],
                si_send.at[i], si_recv.at[i], at(z, x, t2),
            )

        def shared_inner():
            for i in range(len(TP_FLIPS)):
                _, t2 = mate(0, TP_FLIPS[i])
                remote(
                    hblk.at[z], hg.at[:, columns(t2, features)], hg_send.at[i], hg_recv.at[i],
                    at(z, x, t2),
                ).wait_recv()
            hg_own.wait()
            for start in (0, half):
                span_rows = slice(start, start + half)
                normalize(hg[span_rows, :], lambda part: res[span_rows, part])
                own_hid[span_rows, :] = hs[:, columns(t, quarter)]
                si[span_rows, columns(t, shared_units)] = glu(sg, su)
            for i in range(len(TP_FLIPS)):
                inner_copy(i).start()

        def shared_out():
            for i in range(len(TP_FLIPS)):
                _, t2 = mate(0, TP_FLIPS[i])
                remote(
                    si.at[:, columns(t, shared_units)], si.at[:, columns(t2, shared_units)],
                    si_send.at[i], si_recv.at[i], at(z, x, t2),
                ).wait_recv()
                remote(
                    sd_hbm.at[:, columns(t2, quarter)],
                    sdq.at[pl.ds(pl.multiple_of(t2 * shared_units, 16), shared_units)],
                    sd_send.at[i], sd_recv.at[i], at(z, x, t2),
                ).wait_recv()
            sd_own.wait()
            base[...] = own_hid[...].astype(f32) + jnp.dot(
                si[...], sdq[...], preferred_element_type=f32
            )

        pass_heads(1)
        lax.fori_loop(0, count, weigh, 0)
        for load in loads:
            load.wait()
        expert(0)
        pass_heads(2)
        expert(1)
        pass_heads(3)
        shared_inner()
        expert(3)
        expert(2)
        shared_out()

        cuts = [slice(start, start + 256) for start in range(0, quarter, 256)]

        def down_hop(b, c, down):
            return remote(
                passed.at[b, :, cuts[c]], arrived.at[down, b, :, cuts[c]],
                zr_send.at[b, c], zr_recv.at[down, b, c],
                at(z + (-1 if down else 1), x, t),
            )

        def owner_copy(c, i):
            _, t2 = mate(0, TP_FLIPS[i])
            rows = pl.ds(pl.multiple_of(t2 * rows_each, 16), rows_each)
            return remote(
                fin.at[rows, cuts[c]],
                out_ref.at[:, pl.ds(pl.multiple_of(t * quarter + 256 * c, 128), 256)],
                f_send.at[c, i], f_recv.at[c, i], at(z, x, t2),
            )

        def owner_own(c):
            rows = pl.ds(pl.multiple_of(t * rows_each, 16), rows_each)
            return pltpu.make_async_copy(
                fin.at[rows, cuts[c]],
                out_ref.at[:, pl.ds(pl.multiple_of(t * quarter + 256 * c, 128), 256)],
                f_recv.at[c, len(TP_FLIPS)],
            )

        def combine(k):
            b = nearest(k)
            for i in range(len(FLIPS)):
                x2, t2 = mate(*FLIPS[i])
                remote(
                    ret.at[0, :, columns(t2, quarter)], rr.at[b, x2 * tp_count + t2],
                    rt_send.at[b, i], rt_recv.at[b, i], at(z, x2, t2),
                ).wait_recv()
            back_own(b).wait()
            sel_t[...] = sel[b, :, 0:tokens].T
            for c, cut in enumerate(cuts):
                @pl.when((z >= b) & (z < planes - 1))
                def _():
                    down_hop(b, c, 1).wait_recv()

                @pl.when((z <= b) & (z > 0))
                def _():
                    down_hop(b, c, 0).wait_recv()

                total = jnp.dot(
                    sel_t[...], rr[b, :, :, cut].reshape(slots, 256), preferred_element_type=f32
                )
                total = total + arrived[1, b, :, cut].astype(f32)
                total = total + arrived[0, b, :, cut].astype(f32)
                if k:
                    passed[b, :, cut] = total.astype(bf16)

                    @pl.when(z > b)
                    def _():
                        down_hop(b, c, 1).start()

                    @pl.when(z < b)
                    def _():
                        down_hop(b, c, 0).start()
                else:
                    fin[:, cut] = (total + base[:, cut]).astype(bf16)
                    for i in range(len(TP_FLIPS)):
                        owner_copy(c, i).start()
                    owner_own(c).start()

        for k in range(planes - 1, -1, -1):
            combine(k)

        for c in range(len(cuts)):
            for i in range(len(TP_FLIPS)):
                _, t2 = mate(0, TP_FLIPS[i])
                remote(
                    fin.at[0:rows_each, cuts[c]],
                    out_ref.at[:, pl.ds(pl.multiple_of(t2 * quarter + 256 * c, 128), 256)],
                    f_send.at[c, i], f_recv.at[c, i], at(z, x, t2),
                ).wait_recv()
            owner_own(c).wait()

        for step in range(1, planes):
            along(step).wait_send()
        for k in range(planes):
            b = nearest(k)
            across(b).wait_send()
            for up in (1, 0):
                @pl.when(goes(b, up))
                def _():
                    z_hop(rblk, b, up, rz_send, rz_recv).wait_send()
                    z_hop(hblk, b, up, hz_send, hz_recv).wait_send()
            for i in range(len(FLIPS)):
                deal_copy(b, *resid_path[1:], i).wait_send()
                deal_copy(b, *heads_path[1:], i).wait_send()
                back_copy(b, 0, i).wait_send()
            if k:
                for c in range(len(cuts)):
                    down_hop(b, c, 0).wait_send()
        for i in range(len(TP_FLIPS)):
            sd_copies[i].wait_send()
            gather(i).wait_send()
            inner_copy(i).wait_send()
            for c in range(len(cuts)):
                owner_copy(c, i).wait_send()

    vmem = pl.BlockSpec(memory_space=pltpu.VMEM)
    anywhere = pl.BlockSpec(memory_space=pl.ANY)
    dma = pltpu.SemaphoreType.DMA
    flips, tps = len(FLIPS), len(TP_FLIPS)
    cut_count = quarter // 256
    return pl.pallas_call(
        kernel,
        out_shape=jax.ShapeDtypeStruct((rows_each, model), bf16),
        in_specs=[vmem] * 4 + [anywhere] * 8,
        out_specs=vmem,
        scratch_shapes=[
            pltpu.VMEM((count,) + packet.shape, bf16),
            pltpu.VMEM((1, span), f32),
            pltpu.VMEM((1, span), f32),
            pltpu.VMEM((HEAD_SIZE, span), f32),
            pltpu.VMEM((lanes, lanes), bf16),
            pltpu.VMEM((group, lanes), f32),
            pltpu.VMEM((count, capacity, 128), f32),
            pltpu.VMEM((planes, slots, lanes), bf16),
            pltpu.VMEM((tokens, slots), bf16),
            pltpu.VMEM((planes, tokens, quarter), bf16),
            pltpu.VMEM((planes, tokens, features), bf16),
            pltpu.VMEM((planes, slots, quarter), bf16),
            pltpu.VMEM((planes, slots, features), bf16),
            pltpu.VMEM((count, capacity, model), bf16),
            pltpu.VMEM((count, capacity, tp_count * features), bf16),
            pltpu.VMEM((pair, model), bf16),
            pltpu.VMEM((pair, model), bf16),
            pltpu.VMEM((count, capacity, model), bf16),
            pltpu.VMEM((planes, group, capacity, quarter), bf16),
            pltpu.VMEM((planes, tokens, quarter), bf16),
            pltpu.VMEM((2, planes, tokens, quarter), bf16),
            pltpu.VMEM((tokens, quarter), f32),
            pltpu.VMEM((tokens, quarter), bf16),
            pltpu.VMEM((tokens, tp_count * features), bf16),
            pltpu.VMEM((tokens, quarter), bf16),
            pltpu.VMEM((tokens, tp_count * shared_units), bf16),
            pltpu.VMEM((tp_count * shared_units, quarter), bf16),
            pltpu.VMEM(residual.shape, bf16),
            pltpu.VMEM(out_proj.shape, bf16),
            pltpu.VMEM(gate_w.shape, bf16),
            pltpu.VMEM(up_w.shape, bf16),
            pltpu.VMEM(down_w.shape, bf16),
            pltpu.VMEM(shared_gate.shape, bf16),
            pltpu.VMEM(shared_up.shape, bf16),
            dma((7,)),
            dma((2,)),
            dma((planes,)),
            dma((planes,)),
            dma((count,)),
            dma((2, planes)),
            dma((planes,)),
            dma((planes, flips)),
            dma((planes, flips + 1)),
            dma((2, planes)),
            dma((planes,)),
            dma((planes, flips)),
            dma((planes, flips + 1)),
            dma((tps,)),
            dma((tps + 1,)),
            dma((tps,)),
            dma((tps + 1,)),
            dma((tps,)),
            dma((tps,)),
            dma((planes, flips)),
            dma((planes, flips + 1)),
            dma((planes, cut_count)),
            dma((2, planes, cut_count)),
            dma((cut_count, tps)),
            dma((cut_count, tps + 1)),
        ],
        compiler_params=pltpu.CompilerParams(
            collective_id=call_id, has_side_effects=True, vmem_limit_bytes=63 * 1024 * 1024
        ),
        name="whole_layer",
    )(queries_t, packet, gain, ffn_gain, residual, *weights)


def scan_attention(query_rows, key_blocks, score_scale):
    start_state = (
        jnp.full((query_rows.shape[0],), -1e30, jnp.float32),
        jnp.zeros((query_rows.shape[0],), jnp.float32),
        jnp.zeros(query_rows.shape, jnp.float32),
    )

    def step(carry, key_slab):
        run_max, run_total, run_acc = carry
        scores = (
            lax.dot_general(
                query_rows,
                key_slab[:, :HEAD_SIZE],
                (((1,), (1,)), ((), ())),
                preferred_element_type=jnp.float32,
            )
            * score_scale
        )
        new_max = jnp.maximum(run_max, jnp.max(scores, axis=1))
        factor = jnp.exp(run_max - new_max)
        expo_terms = jnp.exp(scores - new_max[:, None])
        new_total = run_total * factor + jnp.sum(expo_terms, axis=1)
        new_acc = run_acc * factor[:, None] + jnp.dot(
            expo_terms.astype(jnp.bfloat16),
            key_slab[:, HEAD_SIZE:],
            preferred_element_type=jnp.float32,
        )
        return ((new_max, new_total, new_acc), None)

    (_, run_total, run_acc), _ = lax.scan(step, start_state, key_blocks)
    return run_acc / run_total[:, None]


def slot_ranks(member):
    order = jnp.arange(member.shape[0], dtype=jnp.int32)
    before = (order[:, None] > order[None, :]).astype(jnp.bfloat16)
    rank = jnp.dot(before, member.astype(jnp.bfloat16), preferred_element_type=jnp.float32)
    return jnp.where(member, rank.astype(jnp.int32), -1)


def expert_block(flat_rows, gate_local, up_local, down_local):
    gate_out = jnp.dot(flat_rows, gate_local, preferred_element_type=jnp.float32)
    up_out = jnp.dot(flat_rows, up_local, preferred_element_type=jnp.float32)
    expert_inner = (jax.nn.silu(gate_out) * up_out).astype(jnp.bfloat16)
    return jnp.dot(expert_inner, down_local, preferred_element_type=jnp.float32).astype(
        jnp.bfloat16
    )


def local(
    queries,
    key_matrix,
    values,
    query_gain,
    key_norm_gain,
    head_gain,
    out_proj,
    residual,
    ffn_gain,
    routes,
    route_weights,
    expert_gate,
    expert_up,
    expert_down,
    shared_gate,
    shared_up,
    shared_down,
):
    tok_count = queries.shape[0]
    head_count = queries.shape[1] // HEAD_SIZE
    sp_count = lax.axis_size("sp")
    tp_count = lax.axis_size("tp")
    tp_index = lax.axis_index("tp")
    sequence_total = tok_count * sp_count
    positions = lax.axis_index("sp") * tok_count + jnp.arange(tok_count, dtype=jnp.int32)
    cosine_table, sine_table = grid_tables(positions, sequence_total)
    rotated_query = apply_rotary(
        final_norm(
            queries.astype(jnp.float32).reshape(tok_count, head_count, HEAD_SIZE), query_gain
        ),
        cosine_table,
        sine_table,
    ).astype(jnp.bfloat16)
    rotated_key = (
        apply_rotary(
            final_norm(
                key_matrix.astype(jnp.float32).reshape(tok_count, 1, HEAD_SIZE), key_norm_gain
            ),
            cosine_table,
            sine_table,
        )
        .reshape(tok_count, HEAD_SIZE)
        .astype(jnp.bfloat16)
    )
    packed = jnp.concatenate([rotated_key, values], axis=1)
    score_scale = HEAD_SIZE ** (-0.5)
    topk_count = routes.shape[1]
    capacity = max(2, 2 * tok_count * topk_count // (sp_count * tp_count))
    lanes = 2 * HEAD_SIZE
    entries = tok_count * topk_count
    relayed = (
        tp_count == 4
        and sp_count == 2 * tp_count
        and capacity % 16 == 0
        and tok_count % (16 * tp_count) == 0
        and entries % lanes == 0
        and head_count * tok_count % 256 == 0
        and head_count % 2 == 0
    )
    if relayed:
        lane_total = -(-tok_count // 128) * 128
        scale_hi = lax.reduce_precision(route_weights, 8, 7)
        tables = jnp.concatenate(
            [routes.astype(jnp.float32), scale_hi, route_weights - scale_hi], axis=1
        ).T
        tables = jnp.pad(
            tables, ((0, -3 * topk_count % 16), (0, lane_total - tok_count)), constant_values=-1.0
        ).astype(jnp.bfloat16)
        tables = tables.reshape(tables.shape[0], -1, 128).transpose(1, 0, 2).reshape(-1, 128)
        scaled = rotated_query * jnp.asarray(score_scale, jnp.bfloat16)
        return whole_layer(
            scaled.transpose(2, 1, 0).reshape(HEAD_SIZE, head_count * tok_count),
            jnp.concatenate([packed, tables], axis=0),
            head_gain.reshape(head_count, HEAD_SIZE),
            ffn_gain.reshape(1, -1),
            residual,
            (out_proj, expert_gate[0], expert_up[0], expert_down[0], shared_gate, shared_up, shared_down),
            tok_count,
            capacity,
            topk_count,
            sp_count // tp_count,
            tp_count,
            0,
        )
    piece = exchange(packed, "sp", 0, True).reshape(sequence_total, lanes)
    query_rows = rotated_query.transpose(1, 0, 2).reshape(head_count * tok_count, HEAD_SIZE)
    block_length = key_block_rows(sequence_total)
    key_blocks = piece.reshape(sequence_total // block_length, block_length, lanes)
    attended = scan_attention(query_rows, key_blocks, score_scale)
    attended = attended.reshape(head_count, tok_count, HEAD_SIZE).transpose(1, 0, 2)
    head_out = final_norm(attended, head_gain.reshape(head_count, HEAD_SIZE))
    head_out = head_out.astype(jnp.bfloat16).reshape(tok_count, head_count * HEAD_SIZE)
    part_rows = tok_count // tp_count
    token_heads = exchange(
        head_out.reshape(tp_count, part_rows, head_count * HEAD_SIZE), "tp", 1, False
    )
    token_heads = token_heads.transpose(1, 0, 2).reshape(part_rows, -1)
    own_resid = lax.dynamic_slice_in_dim(residual, tp_index * part_rows, part_rows, 0)
    hidden_own = (
        own_resid.astype(jnp.float32)
        + jnp.dot(token_heads, out_proj, preferred_element_type=jnp.float32)
    ).astype(jnp.bfloat16)
    normed_own = final_norm(hidden_own.astype(jnp.float32), ffn_gain).astype(jnp.bfloat16)
    model_width = normed_own.shape[1]
    gate_local = expert_gate[0]
    up_local = expert_up[0]
    down_local = expert_down[0]
    normed = exchange(normed_own, "tp", 2, True).reshape(tok_count, model_width)
    slot_total = sp_count * capacity
    experts_here = jnp.arange(sp_count, dtype=jnp.int32) * tp_count + tp_index
    named = routes[:, :, None] == experts_here[None, None, :]
    member = jnp.any(named, axis=1)
    scale = jnp.sum(jnp.where(named, route_weights[:, :, None], 0.0), axis=1)
    rank = slot_ranks(member)
    slots = jnp.arange(capacity, dtype=jnp.int32)
    chosen = rank.T[:, None, :] == slots[None, :, None]
    select = chosen.astype(jnp.bfloat16).reshape(slot_total, tok_count)
    outgoing = jnp.dot(select, normed, preferred_element_type=jnp.float32).astype(jnp.bfloat16)
    arrived = exchange(outgoing.reshape(sp_count, capacity, model_width), "sp", 3, False)
    produced = expert_block(
        arrived.reshape(slot_total, model_width), gate_local, up_local, down_local
    )
    returned = exchange(produced.reshape(sp_count, capacity, model_width), "sp", 4, False).reshape(
        slot_total, model_width
    )
    combine = jnp.where(chosen, scale.T[:, None, :], 0.0).reshape(slot_total, tok_count)
    combine_hi = lax.reduce_precision(combine, 8, 7)
    combine_lo = (combine - combine_hi).astype(jnp.bfloat16)
    combine_hi = combine_hi.astype(jnp.bfloat16)

    def mix(weights):
        return lax.dot_general(
            weights, returned, (((0,), (0,)), ((), ())), preferred_element_type=jnp.float32
        )

    gate_part = jnp.dot(normed, shared_gate, preferred_element_type=jnp.float32)
    up_part = jnp.dot(normed, shared_up, preferred_element_type=jnp.float32)
    shared_inner = (jax.nn.silu(gate_part) * up_part).astype(jnp.bfloat16)
    shares = (
        jnp.dot(shared_inner, shared_down, preferred_element_type=jnp.float32)
        + mix(combine_hi)
        + mix(combine_lo)
    ).astype(jnp.bfloat16)
    shares = exchange(shares.reshape(tp_count, part_rows, model_width), "tp", 5, False)
    mixed_rows = jnp.sum(shares.astype(jnp.float32), axis=0)
    return (hidden_own.astype(jnp.float32) + mixed_rows).astype(jnp.bfloat16)


def solution(mesh):
    placed = (
        P("sp", "tp"),
        P("sp", "tp"),
        P("sp", "tp"),
        P(),
        P(),
        P("tp"),
        P(),
        P("sp", None),
        P(),
        P("sp", None),
        P("sp", None),
        P(("sp", "tp"), None, None),
        P(("sp", "tp"), None, None),
        P(("sp", "tp"), None, None),
        P(None, "tp"),
        P(None, "tp"),
        P("tp", None),
    )
    return jax.shard_map(
        local, mesh=mesh, in_specs=placed, out_specs=P(("sp", "tp"), None), check_vma=False
    )
```

time: 194 us -> 143 us (0.74); the launches traced: 191 us -> 143 us
  Pallas kernels: 156 us -> 136 us
  matrix products: 15.7 us -> 0 us
  other arithmetic: 6.89 us -> 1.65 us
  starting transfers between devices: 5.09 us -> 0 us
    pallas_call x3 -> x1, Pallas kernels: 156 us -> 136 us  [whole_layer(): pl.pallas_call(kernel, out_shape=jax.ShapeDtypeStruct((rows_each, model),...]
    dot_general x4 -> x0, matrix products: 15.7 us -> none  [the longest x1 7.28 us: expert_block(): jnp.dot(expert_inner, down_local, preferred_element_type=jnp.float32)]
    ppermute x3 -> x0, starting transfers between devices: 5.09 us -> none  [across_pairs(): return lax.ppermute(shard, 'tp', [(i, i ^ 2) for i in range(tp_count)])]
    convert_element_type x4 -> x0, other arithmetic: 3.83 us -> none  [the longest x1 1.98 us: local(): return (hidden_own.astype(jnp.float32) + (shared_out + routed.astype(jnp....]
  transfers between devices with their start and end apart: 3 -> 0, of which waited for: 0 -> 0; matrix products, arithmetic and copies ran while one was open for 7% -> 0% of each run, Pallas kernels for 15% -> 0%
where the time goes in v1:
time: 143 us
  Pallas kernels  136 us (95%)
  local copies, waits for them, and re-layouts  5.53 us (4%)
  other arithmetic  1.65 us (1%)
    pallas_call x1, Pallas kernels, whole_layer(): pl.pallas_call(kernel, out_shape=jax.ShapeDtypeStruct((rows_each, model),...  136 us
    unnamed x15, local copies, waits for them, and re-layouts  2.95 us

profile of v1, /device:TPU:0, one launch (start us, length us, event | category | flops | bytes accessed | tf_op | source)
XLA Modules:
  0.0 142.9 jit_solution(3611698060783942623)
XLA Ops:
  0.0 0.0 copy-start.2
  0.0 0.0 copy-start.3
  0.0 0.0 copy-start.1
  0.0 0.0 copy-start
  0.0 0.0 copy-start.5
  0.0 0.8 mul.180
  0.8 1.1 copy.24
  1.9 0.0 copy-start.4
  1.9 0.1 bitcast_reduce_fusion
  2.0 0.1 multiply_multiply_fusion
  2.1 0.1 fusion.6
  2.2 0.2 fusion.5
  2.4 0.1 subtract_convert_fusion
  2.5 0.2 copy.30
  2.7 0.8 reshape.362.q_ref
  3.5 0.0 copy-done.2
  3.5 0.0 copy-done.3
  3.6 0.0 copy-done.1
  3.6 0.1 copy.27
  3.7 0.0 copy-done
  3.8 0.0 copy-done.5
  3.8 0.1 fusion.1
  3.9 0.2 subtract_convert_fusion.1
  4.1 0.1 copy.26
  4.2 0.7 pad_maximum_fusion.own_ref
  5.0 0.0 copy-done.4
  5.0 0.7 reshape.366.gain_ref
  5.6 135.6 %whole_layer.1 = bf16[80,2048]{1,0:T(8,128)(2,1)} custom-call(bf16[64,1280]{1,0:T(8,128)(2,1)} %reshape.362.q_ref, bf16[368,128]{1,0:T(8,128)(2,1)} %pad_maximum_fusion.own_ref, f32[4,64]{1,0:T(4,128)} %reshape.366.gain_ref, f32[1,2048]{1,0:T(1,128)} %bitcast.36, bf16[320,2048]{1,0:T(8,128)(2,1)} %resid_ref.1, bf16[1024,2048]{1,0:T(8,128)(2,1)} %wo_hbm.1, ...), custom_call_target="tpu_custom_call" | custom-call | tf_op jit(solution)/shard_map/whole_layer/pallas_call | solution.py:644
  141.2 1.7 %copy.32 = bf16[80,2048]{1,0:T(8,128)(2,1)} copy(bf16[80,2048]{1,0:T(8,128)(2,1)} %whole_layer.1) | data formatting | bytes 655360
  (13 shorter events, 0.2 us)
Async XLA Ops:
  0.0 3.5 %copy-start.2 = (f32[320,4]{0,1:T(4,128)S(1)}, f32[320,4]{0,1:T(4,128)}, u32[]{:S(2)}) copy-start(f32[320,4]{0,1:T(4,128)} %param.27) | copy-start | bytes 15364
  0.0 3.5 %copy-start.3 = (s32[320,4]{0,1:T(4,128)S(1)}, s32[320,4]{0,1:T(4,128)}, u32[]{:S(2)}) copy-start(s32[320,4]{0,1:T(4,128)} %param.26) | copy-start | bytes 15364
  0.0 3.6 %copy-start.1 = (bf16[320,64]{0,1:T(8,128)(2,1)S(1)}, bf16[320,64]{0,1:T(8,128)(2,1)}, u32[]{:S(2)}) copy-start(bf16[320,64]{0,1:T(8,128)(2,1)} %param.19) | copy-start | bytes 122884
  0.0 3.7 %copy-start = (bf16[320,64]{0,1:T(8,128)(2,1)S(1)}, bf16[320,64]{0,1:T(8,128)(2,1)}, u32[]{:S(2)}) copy-start(bf16[320,64]{0,1:T(8,128)(2,1)} %param.18) | copy-start | bytes 122884
  0.0 3.8 %copy-start.5 = (f32[64]{0:T(128)S(1)}, f32[64]{0:T(128)}, u32[]{:S(2)}) copy-start(f32[64]{0:T(128)} %param.21) | copy-start | bytes 772
  1.9 3.1 %copy-start.4 = (f32[256]{0:T(256)S(1)}, f32[256]{0:T(256)}, u32[]{:S(2)}) copy-start(f32[256]{0:T(256)} %param.22) | copy-start | bytes 3076

commit v2 on v1

--- a/solution.py
+++ b/solution.py
@@ -119,7 +119,8 @@
 
 def whole_layer(
     queries_t,
-    packet,
+    own_kv,
+    own_table,
     gain,
     ffn_gain,
     residual,
@@ -143,7 +144,7 @@
     chunk = 256
     lane_groups = -(-tokens // 128)
     lanes = 128 * lane_groups
-    table_rows = packet.shape[0] - tokens
+    table_rows = own_table.shape[0]
     table_step = table_rows // lane_groups
     slots = group * capacity
     out_proj, gate_w, up_w, down_w, shared_gate, shared_up, shared_down = weights
@@ -154,12 +155,12 @@
     bf16, f32 = jnp.bfloat16, jnp.float32
 
     def kernel(
-        q_ref, own_ref, gain_ref, ffn_ref, resid_ref, wo_hbm, wg_hbm, wu_hbm, wd_hbm,
+        q_ref, own_ref, tab_ref, gain_ref, ffn_ref, resid_ref, wo_hbm, wg_hbm, wu_hbm, wd_hbm,
         sg_hbm, su_hbm, sd_hbm, out_ref,
-        kv, top, norm, acc, tri, ranks, scales, sel, sel_t, rblk, hblk, rpack, hpack,
+        kv, tabs, top, norm, acc, tri, ranks, scales, sel, sel_t, rblk, hblk, rpack, hpack,
         xr, xh, hs, ns, ret, rr, passed, arrived, base, fin, hg, own_hid, si, sdq,
         res, wo, wg, wu, wd, sg, su,
-        w_sem, k_sem, kz_send, kx_send, k_recv,
+        w_sem, k_sem, tb_send, tb_recv, kz_send, kx_send, k_recv,
         rz_send, rz_recv, ri_send, ri_recv, hz_send, hz_recv, hi_send, hi_recv,
         hg_send, hg_recv, sd_send, sd_recv, si_send, si_recv,
         rt_send, rt_recv, zr_send, zr_recv, f_send, f_recv,
@@ -191,17 +192,22 @@
         for dx, dt in FLIPS:
             pl.semaphore_signal(barrier, inc=1, device_id=at(z, *mate(dx, dt)), device_id_type=MESH)
         for step in range(1, planes):
-            pl.semaphore_signal(
-                barrier, inc=1, device_id=at(lax.rem(z + step, planes), x, t), device_id_type=MESH
-            )
+            for x2 in (x, 1 - x):
+                pl.semaphore_signal(
+                    barrier, inc=1, device_id=at(lax.rem(z + step, planes), x2, t),
+                    device_id_type=MESH,
+                )
 
         def columns(index, size):
             return pl.ds(pl.multiple_of(index * size, 128), size)
 
-        kept = pltpu.make_async_copy(own_ref, kv.at[me], k_sem.at[0])
-        kept.start()
-        mine = pltpu.make_async_copy(resid_ref.at[:, columns(t, quarter)], rblk.at[z], k_sem.at[1])
-        mine.start()
+        locals_ = [
+            pltpu.make_async_copy(resid_ref.at[:, columns(t, quarter)], rblk.at[z], k_sem.at[1]),
+            pltpu.make_async_copy(own_ref, kv.at[me], k_sem.at[0]),
+            pltpu.make_async_copy(tab_ref, tabs.at[me], k_sem.at[2]),
+        ]
+        for copy in locals_:
+            copy.start()
         loads = [
             pltpu.make_async_copy(source, target, w_sem.at[i])
             for i, (source, target) in enumerate(
@@ -211,23 +217,27 @@
                 ]
             )
         ]
-        for load in loads:
-            load.start()
         before = lax.broadcasted_iota(jnp.int32, (lanes, lanes), 0)
         after = lax.broadcasted_iota(jnp.int32, (lanes, lanes), 1)
         tri[...] = jnp.where(before < after, 1.0, 0.0).astype(bf16)
-        top[...] = jnp.full(top.shape, -1e30, f32)
-        norm[...] = jnp.zeros(norm.shape, f32)
-        acc[...] = jnp.zeros(acc.shape, f32)
-        kept.wait()
-        mine.wait()
-        pl.semaphore_wait(barrier, len(FLIPS) + planes - 1)
-
-        def along(step):
+        for copy in locals_:
+            copy.wait()
+        pl.semaphore_wait(barrier, len(FLIPS) + 2 * (planes - 1))
+
+        def along(k):
             return remote(
-                own_ref, kv.at[me], kz_send.at[step], k_recv.at[me],
-                at(lax.rem(z + step, planes), x, t),
-            )
+                own_ref, kv.at[me], kz_send.at[k], k_recv.at[me], at(nearest(k), x, t)
+            )
+
+        def table_copy(k, far):
+            i = 2 * k + far
+            return remote(
+                tab_ref, tabs.at[me], tb_send.at[i], tb_recv.at[me],
+                at(nearest(k), 1 - x if far else x, t),
+            )
+
+        def told(slot):
+            return remote(tab_ref, tabs.at[slot], tb_send.at[1], tb_recv.at[slot], at(z, 1 - x, t))
 
         def came(slot):
             return remote(own_ref, kv.at[slot], kz_send.at[0], k_recv.at[slot], at(z, 1 - x, t))
@@ -290,7 +300,7 @@
         heads_path = (hblk, hpack, xh, features, hi_send, hi_recv)
 
         def table(slot):
-            return kv[slot, tokens : tokens + table_rows, :].astype(f32)
+            return tabs[slot].astype(f32)
 
         def index(b):
             rows = table(b * width + x)
@@ -357,10 +367,48 @@
                 )
                 top[:, part] = peak
 
-        for step in range(1, planes):
-            along(step).start()
+        def each_side(step, body):
+            def side_of(i, carry):
+                b = z + (2 * i - 1) * step
+
+                @pl.when((b >= 0) & (b < planes))
+                def _():
+                    body(b)
+
+                return carry
+
+            lax.fori_loop(0, 2, side_of, 0)
+
+        def pass_resid(step):
+            def body(b):
+                z_hop(rblk, b, 0, rz_send, rz_recv).wait_recv()
+                forward(rblk, b, rz_send, rz_recv)
+                told(b * width + x).wait_recv()
+                index(b)
+                deal(b, *resid_path)
+
+            each_side(step, body)
+
+        def pass_heads(step):
+            def body(b):
+                z_hop(hblk, b, 0, hz_send, hz_recv).wait_recv()
+                forward(hblk, b, hz_send, hz_recv)
+                deal(b, *heads_path)
+
+            each_side(step, body)
+
+        for k in range(1, planes):
+            table_copy(k, 0).start()
+        for k in range(1, planes):
+            along(k).start()
         across(z).start()
         forward(rblk, z, rz_send, rz_recv)
+        for k in range(planes):
+            table_copy(k, 1).start()
+        index(z)
+        deal(z, *resid_path)
+        for load in loads:
+            load.start()
         sd_copies = []
         for i, dt in enumerate(TP_FLIPS):
             _, t2 = mate(0, dt)
@@ -369,6 +417,7 @@
                 sdq.at[pl.ds(pl.multiple_of(t * shared_units, 16), shared_units)],
                 sd_send.at[i], sd_recv.at[i], at(z, x, t2),
             )
+            copy.start()
             sd_copies.append(copy)
         sd_own = pltpu.make_async_copy(
             sd_hbm.at[:, columns(t, quarter)],
@@ -376,25 +425,25 @@
             sd_recv.at[len(TP_FLIPS)],
         )
         sd_own.start()
-        index(z)
-        deal(z, *resid_path)
+        top[...] = jnp.full(top.shape, -1e30, f32)
+        norm[...] = jnp.zeros(norm.shape, f32)
+        acc[...] = jnp.zeros(acc.shape, f32)
         absorb(me)
+
+        def attend(k, far):
+            slot = nearest(k) * width + ((1 - x) if far else x)
+            came(slot).wait_recv()
+            if not far:
+                across(nearest(k)).start()
+            absorb(slot)
+
         for k in range(1, planes):
-            b, last = nearest(k), nearest(k - 1)
-            came(b * width + x).wait_recv()
-            across(b).start()
-            index(b)
-            z_hop(rblk, b, 0, rz_send, rz_recv).wait_recv()
-            forward(rblk, b, rz_send, rz_recv)
-            deal(b, *resid_path)
-            came(last * width + (1 - x)).wait_recv()
-            absorb(last * width + (1 - x))
-            absorb(b * width + x)
-        for copy in sd_copies:
-            copy.start()
-        last = nearest(planes - 1)
-        came(last * width + (1 - x)).wait_recv()
-        absorb(last * width + (1 - x))
+            attend(k, False)
+        attend(0, True)
+        attend(1, True)
+        pass_resid(1)
+        attend(2, True)
+        attend(3, True)
 
         attended = acc[...] / norm[...]
         mean_sq = jnp.mean(attended * attended, axis=0, keepdims=True)
@@ -409,23 +458,20 @@
 
         def gather(i):
             _, t2 = mate(0, TP_FLIPS[i])
+            if i == 1:
+                _, t3 = mate(0, 2)
+                _, t2 = mate(0, 1)
+                rows = hg.at[:, columns(t3, features)]
+                return remote(rows, rows, hg_send.at[i], hg_recv.at[i], at(z, x, t2))
             return remote(
                 hblk.at[z], hg.at[:, columns(t, features)], hg_send.at[i], hg_recv.at[i],
                 at(z, x, t2),
             )
 
-        for i in range(len(TP_FLIPS)):
-            gather(i).start()
         hg_own = pltpu.make_async_copy(
             hblk.at[z], hg.at[:, columns(t, features)], hg_recv.at[len(TP_FLIPS)]
         )
         hg_own.start()
-
-        def pass_heads(k):
-            b = nearest(k)
-            z_hop(hblk, b, 0, hz_send, hz_recv).wait_recv()
-            forward(hblk, b, hz_send, hz_recv)
-            deal(b, *heads_path)
 
         def normalize(head_rows, resid_at):
             count_rows = head_rows.shape[0]
@@ -476,6 +522,9 @@
                 part = slice(start, start + COLUMNS)
                 made = jnp.dot(inner_rows, wd[:, part], preferred_element_type=f32) * scale
                 ret[both, :, part] = made.astype(bf16).reshape(width, capacity, COLUMNS)
+
+        def give_back(k):
+            b = nearest(k)
             for i in range(len(FLIPS)):
                 back_copy(b, 0, i).start()
             back_own(b).start()
@@ -494,6 +543,8 @@
                     hblk.at[z], hg.at[:, columns(t2, features)], hg_send.at[i], hg_recv.at[i],
                     at(z, x, t2),
                 ).wait_recv()
+                if i == 0:
+                    gather(1).start()
             hg_own.wait()
             for start in (0, half):
                 span_rows = slice(start, start + half)
@@ -520,18 +571,27 @@
                 si[...], sdq[...], preferred_element_type=f32
             )
 
+        pass_resid(2)
         pass_heads(1)
+        for i in (0, 2):
+            gather(i).start()
+        pass_resid(3)
+        pass_heads(2)
+        pass_heads(3)
+        for step in range(planes):
+            told(step * width + (1 - x)).wait_recv()
         lax.fori_loop(0, count, weigh, 0)
         for load in loads:
             load.wait()
         expert(0)
-        pass_heads(2)
         expert(1)
-        pass_heads(3)
         shared_inner()
+        give_back(1)
         expert(3)
+        give_back(3)
         expert(2)
-        shared_out()
+        give_back(2)
+        give_back(0)
 
         cuts = [slice(start, start + 256) for start in range(0, quarter, 256)]
 
@@ -599,8 +659,10 @@
                         owner_copy(c, i).start()
                     owner_own(c).start()
 
-        for k in range(planes - 1, -1, -1):
+        for k in range(planes - 1, 0, -1):
             combine(k)
+        shared_out()
+        combine(0)
 
         for c in range(len(cuts)):
             for i in range(len(TP_FLIPS)):
@@ -614,9 +676,11 @@
 
         for step in range(1, planes):
             along(step).wait_send()
+            table_copy(step, 0).wait_send()
         for k in range(planes):
             b = nearest(k)
             across(b).wait_send()
+            table_copy(k, 1).wait_send()
             for up in (1, 0):
                 @pl.when(goes(b, up))
                 def _():
@@ -644,10 +708,11 @@
     return pl.pallas_call(
         kernel,
         out_shape=jax.ShapeDtypeStruct((rows_each, model), bf16),
-        in_specs=[vmem] * 4 + [anywhere] * 8,
+        in_specs=[vmem] * 5 + [anywhere] * 8,
         out_specs=vmem,
         scratch_shapes=[
-            pltpu.VMEM((count,) + packet.shape, bf16),
+            pltpu.VMEM((count,) + own_kv.shape, bf16),
+            pltpu.VMEM((count,) + own_table.shape, bf16),
             pltpu.VMEM((1, span), f32),
             pltpu.VMEM((1, span), f32),
             pltpu.VMEM((HEAD_SIZE, span), f32),
@@ -682,7 +747,9 @@
             pltpu.VMEM(shared_gate.shape, bf16),
             pltpu.VMEM(shared_up.shape, bf16),
             dma((7,)),
-            dma((2,)),
+            dma((3,)),
+            dma((2 * planes,)),
+            dma((count,)),
             dma((planes,)),
             dma((planes,)),
             dma((count,)),
@@ -711,7 +778,7 @@
             collective_id=call_id, has_side_effects=True, vmem_limit_bytes=63 * 1024 * 1024
         ),
         name="whole_layer",
-    )(queries_t, packet, gain, ffn_gain, residual, *weights)
+    )(queries_t, own_kv, own_table, gain, ffn_gain, residual, *weights)
 
 
 def scan_attention(query_rows, key_blocks, score_scale):
@@ -836,7 +903,8 @@
         scaled = rotated_query * jnp.asarray(score_scale, jnp.bfloat16)
         return whole_layer(
             scaled.transpose(2, 1, 0).reshape(HEAD_SIZE, head_count * tok_count),
-            jnp.concatenate([packed, tables], axis=0),
+            packed,
+            tables,
             head_gain.reshape(head_count, HEAD_SIZE),
             ffn_gain.reshape(1, -1),
             residual,

time: 143 us -> 127 us (0.89)
  Pallas kernels: 136 us -> 119 us
    pallas_call x1, Pallas kernels: 136 us -> 119 us  [whole_layer(): pl.pallas_call(kernel, out_shape=jax.ShapeDtypeStruct((rows_each, model),...]
where the time goes in v2:
time: 127 us
  Pallas kernels  119 us (94%)
  local copies, waits for them, and re-layouts  6.12 us (5%)
  other arithmetic  1.65 us (1%)
    pallas_call x1, Pallas kernels, whole_layer(): pl.pallas_call(kernel, out_shape=jax.ShapeDtypeStruct((rows_each, model),...  119 us
    unnamed x15, local copies, waits for them, and re-layouts  2.97 us

profile of v2, /device:TPU:0, one launch (start us, length us, event | category | flops | bytes accessed | tf_op | source)
XLA Modules:
  0.0 127.0 jit_solution(14514988076899902987)
XLA Ops:
  0.0 0.0 copy-start.1
  0.0 0.0 copy-start
  0.0 0.0 copy-start.5
  0.0 0.7 mul.180
  0.8 0.0 copy-start.2
  0.8 0.0 copy-start.3
  0.8 1.1 copy.24
  1.9 0.0 copy-start.4
  1.9 0.1 bitcast_reduce_fusion
  2.0 0.1 multiply_multiply_fusion
  2.1 0.1 fusion.6
  2.2 0.2 fusion.5
  2.4 0.1 subtract_convert_fusion
  2.5 0.2 copy.30
  2.6 0.8 reshape.362.q_ref
  3.5 0.0 copy-done.1
  3.5 0.1 copy.27
  3.6 0.0 copy-done
  3.7 0.0 copy-done.5
  3.7 0.1 fusion.1
  3.8 0.2 subtract_convert_fusion.1
  4.0 0.1 copy.26
  4.1 0.7 pad_maximum_fusion.own_ref
  4.8 0.0 copy-done.2
  4.8 0.0 copy-done.3
  4.9 0.6 copy.28
  5.5 0.0 copy-done.4
  5.5 0.7 reshape.366.gain_ref
  6.2 119.1 %whole_layer.1 = bf16[80,2048]{1,0:T(8,128)(2,1)} custom-call(bf16[64,1280]{1,0:T(8,128)(2,1)} %reshape.362.q_ref, bf16[320,128]{1,0:T(8,128)(2,1)} %pad_maximum_fusion.own_ref, bf16[48,128]{1,0:T(8,128)(2,1)} %bitcast.35, f32[4,64]{1,0:T(4,128)} %reshape.366.gain_ref, f32[1,2048]{1,0:T(1,128)} %bitcast.36, bf16[320,2048]{1,0:T(8,128)(2,1)} %resid_ref.1, ...), custom_call_target="tpu_custom_call" | custom-call | tf_op jit(solution)/shard_map/whole_layer/pallas_call | solution.py:708
  125.3 1.7 %copy.32 = bf16[80,2048]{1,0:T(8,128)(2,1)} copy(bf16[80,2048]{1,0:T(8,128)(2,1)} %whole_layer.1) | data formatting | bytes 655360
  (12 shorter events, 0.2 us)
Async XLA Ops:
  0.0 3.5 %copy-start.1 = (bf16[320,64]{0,1:T(8,128)(2,1)S(1)}, bf16[320,64]{0,1:T(8,128)(2,1)}, u32[]{:S(2)}) copy-start(bf16[320,64]{0,1:T(8,128)(2,1)} %param.19) | copy-start | bytes 122884
  0.0 3.6 %copy-start = (bf16[320,64]{0,1:T(8,128)(2,1)S(1)}, bf16[320,64]{0,1:T(8,128)(2,1)}, u32[]{:S(2)}) copy-start(bf16[320,64]{0,1:T(8,128)(2,1)} %param.18) | copy-start | bytes 122884
  0.0 3.7 %copy-start.5 = (f32[64]{0:T(128)S(1)}, f32[64]{0:T(128)}, u32[]{:S(2)}) copy-start(f32[64]{0:T(128)} %param.21) | copy-start | bytes 772
  0.8 4.1 %copy-start.2 = (f32[320,4]{0,1:T(4,128)S(1)}, f32[320,4]{0,1:T(4,128)}, u32[]{:S(2)}) copy-start(f32[320,4]{0,1:T(4,128)} %param.27) | copy-start | bytes 15364
  0.8 4.1 %copy-start.3 = (s32[320,4]{0,1:T(4,128)S(1)}, s32[320,4]{0,1:T(4,128)}, u32[]{:S(2)}) copy-start(s32[320,4]{0,1:T(4,128)} %param.26) | copy-start | bytes 15364
  1.9 3.7 %copy-start.4 = (f32[256]{0:T(256)S(1)}, f32[256]{0:T(256)}, u32[]{:S(2)}) copy-start(f32[256]{0:T(256)} %param.22) | copy-start | bytes 3076

commit v3 on v2

--- a/solution.py
+++ b/solution.py
@@ -136,7 +136,7 @@
     planes = count // width
     group = width * tp_count
     span = queries_t.shape[1]
-    heads = gain.shape[0]
+    heads = gain.shape[1] // HEAD_SIZE
     features = heads * HEAD_SIZE
     model = residual.shape[1]
     quarter = model // tp_count
@@ -450,7 +450,8 @@
         rows = (attended * lax.rsqrt(mean_sq + EPS)).T
         for h in range(heads):
             hblk[z, :, h * HEAD_SIZE : (h + 1) * HEAD_SIZE] = (
-                rows[h * tokens : (h + 1) * tokens] * gain_ref[h : h + 1, :]
+                rows[h * tokens : (h + 1) * tokens]
+                * gain_ref[:, h * HEAD_SIZE : (h + 1) * HEAD_SIZE]
             ).astype(bf16)
 
         forward(hblk, z, hz_send, hz_recv)
@@ -528,6 +529,10 @@
             for i in range(len(FLIPS)):
                 back_copy(b, 0, i).start()
             back_own(b).start()
+
+        def given(k):
+            for i in range(len(FLIPS)):
+                back_copy(nearest(k), 0, i).wait_send()
 
         def inner_copy(i):
             _, t2 = mate(0, TP_FLIPS[i])
@@ -586,12 +591,11 @@
         expert(0)
         expert(1)
         shared_inner()
-        give_back(1)
         expert(3)
         give_back(3)
         expert(2)
+        given(3)
         give_back(2)
-        give_back(0)
 
         cuts = [slice(start, start + 256) for start in range(0, quarter, 256)]
 
@@ -659,8 +663,13 @@
                         owner_copy(c, i).start()
                     owner_own(c).start()
 
-        for k in range(planes - 1, 0, -1):
-            combine(k)
+        combine(3)
+        given(2)
+        give_back(1)
+        combine(2)
+        given(1)
+        give_back(0)
+        combine(1)
         shared_out()
         combine(0)
 
@@ -689,7 +698,8 @@
             for i in range(len(FLIPS)):
                 deal_copy(b, *resid_path[1:], i).wait_send()
                 deal_copy(b, *heads_path[1:], i).wait_send()
-                back_copy(b, 0, i).wait_send()
+                if k == 0:
+                    back_copy(b, 0, i).wait_send()
             if k:
                 for c in range(len(cuts)):
                     down_hop(b, c, 0).wait_send()
@@ -905,7 +915,7 @@
             scaled.transpose(2, 1, 0).reshape(HEAD_SIZE, head_count * tok_count),
             packed,
             tables,
-            head_gain.reshape(head_count, HEAD_SIZE),
+            head_gain.reshape(1, -1),
             ffn_gain.reshape(1, -1),
             residual,
             (out_proj, expert_gate[0], expert_up[0], expert_down[0], shared_gate, shared_up, shared_down),

time: 127 us -> 118 us (0.929)
  Pallas kernels: 119 us -> 110 us
    pallas_call x1, Pallas kernels: 119 us -> 110 us  [whole_layer(): pl.pallas_call(kernel, out_shape=jax.ShapeDtypeStruct((rows_each, model),...]
    unnamed x15 -> x13, local copies, waits for them, and re-layouts: 2.97 us -> 2.97 us
where the time goes in v3:
time: 118 us
  Pallas kernels  110 us (93%)
  local copies, waits for them, and re-layouts  5.45 us (5%)
  other arithmetic  1.65 us (1%)
    pallas_call x1, Pallas kernels, whole_layer(): pl.pallas_call(kernel, out_shape=jax.ShapeDtypeStruct((rows_each, model),...  110 us
    unnamed x13, local copies, waits for them, and re-layouts  2.97 us

profile of v3, /device:TPU:0, one launch (start us, length us, event | category | flops | bytes accessed | tf_op | source)
XLA Modules:
  0.0 117.6 jit_solution(13231923532979049797)
XLA Ops:
  0.0 0.0 copy-start.1
  0.0 0.0 copy-start
  0.0 0.0 copy-start.4
  0.0 0.7 mul.180
  0.8 0.0 copy-start.2
  0.8 0.0 copy-start.3
  0.8 1.1 copy.24
  1.9 0.1 bitcast_reduce_fusion
  1.9 0.1 multiply_multiply_fusion
  2.1 0.1 fusion.6
  2.2 0.2 fusion.5
  2.4 0.1 subtract_convert_fusion
  2.5 0.2 copy.30
  2.6 0.8 reshape.362.q_ref
  3.5 0.0 copy-done.1
  3.5 0.1 copy.27
  3.6 0.0 copy-done
  3.7 0.0 copy-done.4
  3.7 0.1 fusion.1
  3.7 0.2 subtract_convert_fusion.1
  4.0 0.1 copy.26
  4.1 0.7 pad_maximum_fusion.own_ref
  4.8 0.0 copy-done.2
  4.8 0.0 copy-done.3
  4.9 0.6 copy.28
  5.5 110.4 %whole_layer.1 = bf16[80,2048]{1,0:T(8,128)(2,1)} custom-call(bf16[64,1280]{1,0:T(8,128)(2,1)} %reshape.362.q_ref, bf16[320,128]{1,0:T(8,128)(2,1)} %pad_maximum_fusion.own_ref, bf16[48,128]{1,0:T(8,128)(2,1)} %bitcast.36, f32[1,256]{1,0:T(1,128)} %bitcast.38, f32[1,2048]{1,0:T(1,128)} %bitcast.37, bf16[320,2048]{1,0:T(8,128)(2,1)} %resid_ref.1, ...), custom_call_target="tpu_custom_call" | custom-call | tf_op jit(solution)/shard_map/whole_layer/pallas_call | solution.py:718
  115.9 1.7 %copy.32 = bf16[80,2048]{1,0:T(8,128)(2,1)} copy(bf16[80,2048]{1,0:T(8,128)(2,1)} %whole_layer.1) | data formatting | bytes 655360
  (12 shorter events, 0.2 us)
Async XLA Ops:
  0.0 3.5 %copy-start.1 = (bf16[320,64]{0,1:T(8,128)(2,1)S(1)}, bf16[320,64]{0,1:T(8,128)(2,1)}, u32[]{:S(2)}) copy-start(bf16[320,64]{0,1:T(8,128)(2,1)} %param.19) | copy-start | bytes 122884
  0.0 3.6 %copy-start = (bf16[320,64]{0,1:T(8,128)(2,1)S(1)}, bf16[320,64]{0,1:T(8,128)(2,1)}, u32[]{:S(2)}) copy-start(bf16[320,64]{0,1:T(8,128)(2,1)} %param.18) | copy-start | bytes 122884
  0.0 3.6 %copy-start.4 = (f32[64]{0:T(128)S(1)}, f32[64]{0:T(128)}, u32[]{:S(2)}) copy-start(f32[64]{0:T(128)} %param.21) | copy-start | bytes 772
  0.8 4.1 %copy-start.2 = (f32[320,4]{0,1:T(4,128)S(1)}, f32[320,4]{0,1:T(4,128)}, u32[]{:S(2)}) copy-start(f32[320,4]{0,1:T(4,128)} %param.27) | copy-start | bytes 15364
  0.8 4.1 %copy-start.3 = (s32[320,4]{0,1:T(4,128)S(1)}, s32[320,4]{0,1:T(4,128)}, u32[]{:S(2)}) copy-start(s32[320,4]{0,1:T(4,128)} %param.26) | copy-start | bytes 15364

commit v4 on v3

--- a/solution.py
+++ b/solution.py
@@ -597,7 +597,7 @@
         given(3)
         give_back(2)
 
-        cuts = [slice(start, start + 256) for start in range(0, quarter, 256)]
+        cuts = [slice(start, start + 128) for start in range(0, quarter, 128)]
 
         def down_hop(b, c, down):
             return remote(
@@ -611,7 +611,7 @@
             rows = pl.ds(pl.multiple_of(t2 * rows_each, 16), rows_each)
             return remote(
                 fin.at[rows, cuts[c]],
-                out_ref.at[:, pl.ds(pl.multiple_of(t * quarter + 256 * c, 128), 256)],
+                out_ref.at[:, pl.ds(pl.multiple_of(t * quarter + 128 * c, 128), 128)],
                 f_send.at[c, i], f_recv.at[c, i], at(z, x, t2),
             )
 
@@ -619,7 +619,7 @@
             rows = pl.ds(pl.multiple_of(t * rows_each, 16), rows_each)
             return pltpu.make_async_copy(
                 fin.at[rows, cuts[c]],
-                out_ref.at[:, pl.ds(pl.multiple_of(t * quarter + 256 * c, 128), 256)],
+                out_ref.at[:, pl.ds(pl.multiple_of(t * quarter + 128 * c, 128), 128)],
                 f_recv.at[c, len(TP_FLIPS)],
             )
 
@@ -643,7 +643,7 @@
                     down_hop(b, c, 0).wait_recv()
 
                 total = jnp.dot(
-                    sel_t[...], rr[b, :, :, cut].reshape(slots, 256), preferred_element_type=f32
+                    sel_t[...], rr[b, :, :, cut].reshape(slots, 128), preferred_element_type=f32
                 )
                 total = total + arrived[1, b, :, cut].astype(f32)
                 total = total + arrived[0, b, :, cut].astype(f32)
@@ -678,7 +678,7 @@
                 _, t2 = mate(0, TP_FLIPS[i])
                 remote(
                     fin.at[0:rows_each, cuts[c]],
-                    out_ref.at[:, pl.ds(pl.multiple_of(t2 * quarter + 256 * c, 128), 256)],
+                    out_ref.at[:, pl.ds(pl.multiple_of(t2 * quarter + 128 * c, 128), 128)],
                     f_send.at[c, i], f_recv.at[c, i], at(z, x, t2),
                 ).wait_recv()
             owner_own(c).wait()
@@ -714,7 +714,7 @@
     anywhere = pl.BlockSpec(memory_space=pl.ANY)
     dma = pltpu.SemaphoreType.DMA
     flips, tps = len(FLIPS), len(TP_FLIPS)
-    cut_count = quarter // 256
+    cut_count = quarter // 128
     return pl.pallas_call(
         kernel,
         out_shape=jax.ShapeDtypeStruct((rows_each, model), bf16),

time: 118 us -> 117 us (level)
  no operation moved by 1% of the time
where the time goes in v4:
time: 117 us
  Pallas kernels  110 us (94%)
  local copies, waits for them, and re-layouts  5.45 us (5%)
  other arithmetic  1.65 us (1%)
    pallas_call x1, Pallas kernels, whole_layer(): pl.pallas_call(kernel, out_shape=jax.ShapeDtypeStruct((rows_each, model),...  110 us
    unnamed x13, local copies, waits for them, and re-layouts  2.97 us

profile of v4, /device:TPU:0, one launch (start us, length us, event | category | flops | bytes accessed | tf_op | source)
XLA Modules:
  0.0 117.2 jit_solution(9842395617071523105)
XLA Ops:
  0.0 0.0 copy-start.1
  0.0 0.0 copy-start
  0.0 0.0 copy-start.4
  0.0 0.7 mul.180
  0.8 0.0 copy-start.2
  0.8 0.0 copy-start.3
  0.8 1.1 copy.24
  1.9 0.1 bitcast_reduce_fusion
  1.9 0.1 multiply_multiply_fusion
  2.1 0.1 fusion.6
  2.2 0.2 fusion.5
  2.4 0.1 subtract_convert_fusion
  2.5 0.2 copy.30
  2.6 0.8 reshape.362.q_ref
  3.5 0.0 copy-done.1
  3.5 0.1 copy.27
  3.6 0.0 copy-done
  3.7 0.0 copy-done.4
  3.7 0.1 fusion.1
  3.7 0.2 subtract_convert_fusion.1
  4.0 0.1 copy.26
  4.1 0.7 pad_maximum_fusion.own_ref
  4.8 0.0 copy-done.2
  4.8 0.0 copy-done.3
  4.9 0.6 copy.28
  5.5 110.0 %whole_layer.1 = bf16[80,2048]{1,0:T(8,128)(2,1)} custom-call(bf16[64,1280]{1,0:T(8,128)(2,1)} %reshape.362.q_ref, bf16[320,128]{1,0:T(8,128)(2,1)} %pad_maximum_fusion.own_ref, bf16[48,128]{1,0:T(8,128)(2,1)} %bitcast.36, f32[1,256]{1,0:T(1,128)} %bitcast.38, f32[1,2048]{1,0:T(1,128)} %bitcast.37, bf16[320,2048]{1,0:T(8,128)(2,1)} %resid_ref.1, ...), custom_call_target="tpu_custom_call" | custom-call | tf_op jit(solution)/shard_map/whole_layer/pallas_call | solution.py:718
  115.5 1.7 %copy.32 = bf16[80,2048]{1,0:T(8,128)(2,1)} copy(bf16[80,2048]{1,0:T(8,128)(2,1)} %whole_layer.1) | data formatting | bytes 655360
  (12 shorter events, 0.2 us)
Async XLA Ops:
  0.0 3.5 %copy-start.1 = (bf16[320,64]{0,1:T(8,128)(2,1)S(1)}, bf16[320,64]{0,1:T(8,128)(2,1)}, u32[]{:S(2)}) copy-start(bf16[320,64]{0,1:T(8,128)(2,1)} %param.19) | copy-start | bytes 122884
  0.0 3.6 %copy-start = (bf16[320,64]{0,1:T(8,128)(2,1)S(1)}, bf16[320,64]{0,1:T(8,128)(2,1)}, u32[]{:S(2)}) copy-start(bf16[320,64]{0,1:T(8,128)(2,1)} %param.18) | copy-start | bytes 122884
  0.0 3.6 %copy-start.4 = (f32[64]{0:T(128)S(1)}, f32[64]{0:T(128)}, u32[]{:S(2)}) copy-start(f32[64]{0:T(128)} %param.21) | copy-start | bytes 772
  0.8 4.1 %copy-start.2 = (f32[320,4]{0,1:T(4,128)S(1)}, f32[320,4]{0,1:T(4,128)}, u32[]{:S(2)}) copy-start(f32[320,4]{0,1:T(4,128)} %param.27) | copy-start | bytes 15364
  0.8 4.1 %copy-start.3 = (s32[320,4]{0,1:T(4,128)S(1)}, s32[320,4]{0,1:T(4,128)}, u32[]{:S(2)}) copy-start(s32[320,4]{0,1:T(4,128)} %param.26) | copy-start | bytes 15364
